TPU v7x, 256 devices: a 4x2x16 block of a 4x16x16 slice. The times are simulated.
256 devices in a mesh: grp: 2 (over y), ep: 32 (over z, core), tp: 4 (over x).
Axes of the slice: x: 4, y: 2, z: 16, core: 2. Of those that a mesh axis runs over, the one named last changes fastest.
The devices are a block of a 4x16x16 slice.
Arguments:
- query: bfloat16 [65536, 1024], P(('grp', 'ep'), 'tp'), parts along dimension 0, may hold values from -6 to 6
- forget_gate_logits: bfloat16 [65536, 1024], P(('grp', 'ep'), 'tp'), parts along dimension 0, may hold values from -8 to 8
- value: bfloat16 [65536, 1024], P(('grp', 'ep'), 'tp'), parts along dimension 0, may hold values from -6 to 6
- forget_lower_margin: float32 [2, 1024], P(None, 'tp'), may hold values from -30 to -2
- position_log_decay: float32 [8, 65536], P('tp', ('grp', 'ep')), parts along dimension 1, may hold values from -1.5 to 0
- head_norm_gain: float32 [128], replicated, may hold values from 0.1 to 1.9
- mixer_output_weight: bfloat16 [1024, 2048], P('tp'), may hold values from -0.1875 to 0.1875
- second_batch_tokens: bfloat16 [32768, 2048], P(('grp', 'ep', 'tp')), parts along dimension 0, may hold values from -60 to 60
- expert_norm_gain: float32 [2048], replicated, may hold values from 0.1 to 1.9
- routes: int32 [32768, 2], P(('grp', 'ep', 'tp')), parts along dimension 0, may hold values from 0 to 31, all different within a row; in each aligned block of 128 rows (0 to 127, 128 to 255, ...) at most 12 rows name the same one
- chosen_expert_weight: float32 [32768, 2], P(('grp', 'ep', 'tp')), parts along dimension 0, may hold values from 0.2 to 1
- gate_weight: bfloat16 [32, 2048, 2048], P('ep', None, 'tp'), may hold values from -0.3125 to 0.3125
- up_weight: bfloat16 [32, 2048, 2048], P('ep', None, 'tp'), may hold values from -0.3125 to 0.3125
- down_weight: bfloat16 [32, 2048, 2048], P('ep', 'tp'), may hold values from -0.02734375 to 0.02734375
Outputs:
- first_mixer_output: bfloat16 [65536, 2048], P(('grp', 'ep', 'tp')), parts along dimension 0
- moe_out: bfloat16 [32768, 2048], P(('grp', 'ep', 'tp')), parts along dimension 0
There are 2 independent parts, one for each index of `grp`. A program takes and returns all parts, laid end to end along the dimension named above; an argument that names none is the same for every part. Nothing has to cross between parts.
Inputs may be any that keep to these rules, and one draw needn't show every extreme that they name: `routes`: each row names 2 different experts. Among the rows of one device no expert is named by more than 12 rows, and in every draw some expert is named by exactly 12 rows of some device.
All inputs are finite; a program needn't handle non-finite values.
Results may differ from a plain program's by a relative error of at most 0.015.
Values may be sent and summed in bfloat16 or wider, within the bound.
No kernel may reach another device: no remote copies, remote signals or barrier semaphores. Data moves between devices by JAX's collectives and lax.ppermute only.
A program may use at most 128 MiB of HBM per device.

v0:
```python
import functools

import jax
import jax.numpy as jnp
from jax import lax
from jax.experimental import pallas as pl
from jax.experimental.pallas import tpu as pltpu
from jax.sharding import Mesh
from jax.sharding import PartitionSpec as P


HEAD_CHANNELS = 128
BLK = 128
STATE_ROWS = HEAD_CHANNELS + 16
EP = ("ep_0", "ep_1")
GRP_EP = ("grp", "ep_0", "ep_1")
GRP_EP_TP = ("grp", "ep_0", "ep_1", "tp")
TILE = 8

NORM_EPS = 1e-06
CLAMP_LIMIT = 7.0
SIGMOID_SCALE = 1.702

F32 = jnp.float32
BF16 = jnp.bfloat16
SMEM = pl.BlockSpec(memory_space=pltpu.SMEM)
VMEM = pl.BlockSpec(memory_space=pltpu.VMEM)


def mm(a, b, lhs_dim, rhs_dim):
    return lax.dot_general(
        a, b, (((lhs_dim,), (rhs_dim,)), ((), ())), preferred_element_type=F32
    )


def pieces_of(x):
    high = x.astype(BF16)
    rest = x - high.astype(F32)
    middle = rest.astype(BF16)
    low = (rest - middle.astype(F32)).astype(BF16)
    return high, middle, low


def summed_along(triangle, x):
    return sum(mm(triangle, piece, 1, 0) for piece in pieces_of(x))


def triangle_of(size, keep):
    rows = lax.broadcasted_iota(jnp.int32, (size, size), 0)
    columns = lax.broadcasted_iota(jnp.int32, (size, size), 1)
    return keep(rows, columns)


def block_gates(logits, margin, decay_row, triangle):
    closing = jnp.exp(margin) * jax.nn.sigmoid(-logits.astype(F32))
    spikes = jnp.transpose(jnp.broadcast_to(decay_row, (BLK, BLK)))
    return closing, summed_along(triangle, jnp.log1p(-closing) + spikes)


def advanced(state, total, closing, cumul, values):
    key_state = (closing * jnp.exp(total - cumul)).astype(BF16)
    return state * jnp.exp(total) + mm(values, key_state, 0, 0)


def rows_of(block):
    return pl.ds(pl.multiple_of(block * BLK, BLK), BLK)


def columns_of(head):
    return slice(head * HEAD_CHANNELS, (head + 1) * HEAD_CHANNELS)


def states_kernel(logits_ref, value_ref, margin_ref, decay_ref, state_ref):
    blocks = logits_ref.shape[0] // BLK
    heads = state_ref.shape[0]
    triangles = (
        triangle_of(BLK, lambda r, c: r >= c).astype(BF16),
        triangle_of(BLK, lambda r, c: r <= c).astype(BF16),
    )
    chains = [(h, d) for h in range(heads) for d in range(2)]

    def step(i, carry):
        after = []
        for (h, d), (state, log) in zip(chains, carry):
            rows = rows_of(i if d == 0 else blocks - 1 - i)
            closing, cumul = block_gates(
                logits_ref[rows, columns_of(h)],
                margin_ref[d : d + 1, columns_of(h)],
                decay_ref[h : h + 1, rows],
                triangles[d],
            )
            total = cumul[BLK - 1 :, :] if d == 0 else cumul[:1, :]
            state = advanced(state, total, closing, cumul, value_ref[rows, columns_of(h)])
            after.append((state, log + total))
        return tuple(after)

    zero = (jnp.zeros((HEAD_CHANNELS, HEAD_CHANNELS), F32), jnp.zeros((1, HEAD_CHANNELS), F32))
    for (h, d), (state, log) in zip(
        chains, lax.fori_loop(0, blocks, step, (zero,) * len(chains))
    ):
        store_state(state_ref, (h, d), state, log)


def mixer_states(logits, value, margin, decay):
    tokens, channels = logits.shape
    heads = channels // HEAD_CHANNELS
    return pl.pallas_call(
        states_kernel,
        in_specs=[VMEM] * 4,
        out_specs=VMEM,
        out_shape=jax.ShapeDtypeStruct((heads, 2, STATE_ROWS, HEAD_CHANNELS), BF16),
        cost_estimate=pl.CostEstimate(
            flops=24 * tokens * channels * BLK, bytes_accessed=5 * tokens * channels, transcendentals=0
        ),
        name="mixer_states",
    )(logits, value, margin, decay)


def decay_of(block):
    tail = block[HEAD_CHANNELS:, :].astype(F32)
    return tail[0:1, :] + tail[1:2, :] + tail[2:3, :]


def store_state(ref, index, state, log):
    places = lax.broadcasted_iota(jnp.int32, (STATE_ROWS - HEAD_CHANNELS, HEAD_CHANNELS), 0)
    tail = jnp.zeros(places.shape, F32)
    for k, piece in enumerate(pieces_of(log)):
        tail = jnp.where(places == k, piece.astype(F32), tail)
    ref[(*index, slice(0, HEAD_CHANNELS), slice(None))] = state.astype(BF16)
    ref[(*index, slice(HEAD_CHANNELS, STATE_ROWS), slice(None))] = tail.astype(BF16)


def merge_kernel(core_ref, own_ref, partner_ref, chip_ref):
    core = core_ref[0]
    for d in range(2):
        own, partner = own_ref[core, d], partner_ref[core, d]
        own_last = (core == 1) if d == 0 else (core == 0)
        first = jnp.where(own_last, partner.astype(F32), own.astype(F32))
        second = jnp.where(own_last, own.astype(F32), partner.astype(F32))
        state = first[:HEAD_CHANNELS] * jnp.exp(decay_of(second)) + second[:HEAD_CHANNELS]
        store_state(chip_ref, (d,), state, decay_of(first) + decay_of(second))


def merged_states(core, own, partner):
    return pl.pallas_call(
        merge_kernel,
        in_specs=[SMEM, VMEM, VMEM],
        out_specs=VMEM,
        out_shape=jax.ShapeDtypeStruct(own.shape[1:], BF16),
        cost_estimate=pl.CostEstimate(flops=8 * own.size, bytes_accessed=5 * own.size, transcendentals=0),
        name="mixer_merge",
    )(core, own, partner)


def entering_kernel(chip_ref, gathered_ref, out_ref):
    chips = gathered_ref.shape[0]
    chip = chip_ref[0]
    for d in range(2):

        def step(i, state):
            j = i if d == 0 else chips - 1 - i
            passed = (j < chip) if d == 0 else (j > chip)
            block = gathered_ref[j, d]
            later = state * jnp.exp(decay_of(block)) + block[:HEAD_CHANNELS, :].astype(F32)
            return jnp.where(passed, later, state)

        zero = jnp.zeros((HEAD_CHANNELS, HEAD_CHANNELS), F32)
        out_ref[d] = lax.fori_loop(0, chips, step, zero).astype(BF16)


def entering_states(chip, gathered):
    return pl.pallas_call(
        entering_kernel,
        in_specs=[SMEM, VMEM],
        out_specs=VMEM,
        out_shape=jax.ShapeDtypeStruct((2, HEAD_CHANNELS, HEAD_CHANNELS), BF16),
        cost_estimate=pl.CostEstimate(
            flops=8 * gathered.size, bytes_accessed=2 * gathered.size, transcendentals=0
        ),
        name="mixer_entering",
    )(chip, gathered)


def heads_kernel(
    place_ref,
    query_ref,
    logits_ref,
    value_ref,
    margin_ref,
    decay_ref,
    gain_ref,
    mine_ref,
    other_ref,
    partner_ref,
    out_ref,
    part_ref,
):
    blocks = logits_ref.shape[0] // BLK
    owners, heads = out_ref.shape[0], out_ref.shape[1]
    per = out_ref.shape[2] // BLK
    core, me = place_ref[0], place_ref[1]
    chains = [(h, d) for h in range(heads) for d in range(2)]

    def entering(h, d):
        state = jnp.where(core == h, mine_ref[d].astype(F32), other_ref[d].astype(F32))
        block = partner_ref[h, d]
        later = state * jnp.exp(decay_of(block)) + block[:HEAD_CHANNELS, :].astype(F32)
        return jnp.where((core == 1) if d == 0 else (core == 0), later, state)

    def part(block, state, h, d):
        rows = rows_of(block)
        keep = triangle_of(BLK, (lambda r, c: r >= c) if d == 0 else (lambda r, c: r <= c))
        values = value_ref[rows, columns_of(h)]
        closing, cumul = block_gates(
            logits_ref[rows, columns_of(h)],
            margin_ref[d : d + 1, columns_of(h)],
            decay_ref[h : h + 1, rows],
            keep.astype(BF16),
        )
        queries = query_ref[rows, columns_of(h)].astype(F32)
        queries = queries * jax.nn.sigmoid(queries) * HEAD_CHANNELS ** (-0.5)
        query_in = (queries * jnp.exp(cumul)).astype(BF16)
        key_in = (closing * jnp.exp(-cumul)).astype(BF16)
        scores = jnp.where(keep, mm(query_in, key_in, 1, 1), 0.0).astype(BF16)
        part_ref[d, rows, columns_of(h)] = mm(scores, values, 1, 0) + mm(
            query_in, state.astype(BF16), 1, 1
        )
        total = cumul[BLK - 1 :, :] if d == 0 else cumul[:1, :]
        return advanced(state, total, closing, cumul, values)

    def step(i, states):
        return tuple(
            part(i if d == 0 else blocks - 1 - i, state, h, d)
            for (h, d), state in zip(chains, states)
        )

    lax.fori_loop(0, blocks, step, tuple(entering(h, d) for h, d in chains))

    def finish(block, _):
        rows = rows_of(block)
        away = lax.rem(block // per - me + owners, owners)
        part_rows = pl.ds(pl.multiple_of((block % per) * BLK, BLK), BLK)
        for h in range(heads):
            mix = part_ref[0, rows, columns_of(h)] + part_ref[1, rows, columns_of(h)]
            scale = lax.rsqrt(jnp.mean(mix * mix, axis=-1, keepdims=True) + NORM_EPS)
            out_ref[away, h, part_rows, :] = (mix * scale * gain_ref[...]).astype(BF16)
        return 0

    lax.fori_loop(0, blocks, finish, 0)


def mixer_heads(place, query, logits, value, margin, decay, gain, mine, other, partner, owners):
    tokens, channels = logits.shape
    heads = channels // HEAD_CHANNELS
    return pl.pallas_call(
        heads_kernel,
        in_specs=[SMEM] + [VMEM] * 9,
        out_specs=VMEM,
        scratch_shapes=[pltpu.VMEM((2, tokens, channels), F32)],
        out_shape=jax.ShapeDtypeStruct((owners, heads, tokens // owners, HEAD_CHANNELS), BF16),
        cost_estimate=pl.CostEstimate(
            flops=48 * tokens * channels * BLK, bytes_accessed=16 * tokens * channels, transcendentals=0
        ),
        name="mixer_heads",
    )(place, query, logits, value, margin, decay, gain.reshape(1, HEAD_CHANNELS), mine, other, partner)


def project_kernel(place_ref, own_ref, left_ref, right_ref, far_ref, mine_ref, other_ref, out_ref):
    core, me = place_ref[0], place_ref[1]
    owners = mine_ref.shape[0]
    width = 256

    def columns(c, _):
        cols = pl.ds(pl.multiple_of(c * width, width), width)
        total = jnp.zeros((out_ref.shape[0], width), F32)
        for ref, by in ((own_ref, 0), (left_ref, owners - 1), (right_ref, 1), (far_ref, 2)):
            source = lax.rem(me + by, owners)
            total += mm(ref[core], mine_ref[source, :, cols], 1, 0)
            total += mm(ref[1 - core], other_ref[source, :, cols], 1, 0)
        out_ref[:, cols] = total.astype(BF16)
        return 0

    lax.fori_loop(0, out_ref.shape[1] // width, columns, 0)


def project(place, heads, mine, other):
    tokens, features = heads[0].shape[1], mine.shape[2]
    return pl.pallas_call(
        project_kernel,
        in_specs=[SMEM] + [VMEM] * 6,
        out_specs=VMEM,
        out_shape=jax.ShapeDtypeStruct((tokens, features), BF16),
        cost_estimate=pl.CostEstimate(
            flops=8 * heads[0].size * features, bytes_accessed=8 * tokens * features, transcendentals=0
        ),
        name="mixer_project",
    )(place, *heads, mine, other)


def slots_of(routes, core, experts):
    top_count, tokens = routes.shape
    number = lax.broadcasted_iota(jnp.int32, (experts, tokens), 0)
    named = [routes[k : k + 1, :] == number for k in range(top_count)]
    counts = sum(n.astype(F32) for n in named).astype(BF16)
    earlier = triangle_of(tokens, lambda r, c: r < c).astype(BF16)
    ranking = mm(counts, earlier, 1, 0)
    result = []
    for k, n in enumerate(named):
        slot = jnp.sum(jnp.where(n, ranking, 0.0), axis=0, keepdims=True).astype(jnp.int32)
        expert = routes[k : k + 1, :]
        chip = expert // 2
        far = jnp.where(expert - 2 * chip == core, 0, 1)
        late = slot >= TILE
        block = jnp.where(late, 2 + far, far)
        inside = jnp.where(late, slot - TILE + far * (TILE // 2), slot)
        result.append((block, chip * TILE + inside))
    return result


def dispatch_kernel(experts, core_ref, token_ref, gain_ref, route_ref, *send_refs):
    tokens = token_ref[...].astype(F32)
    scale = lax.rsqrt(jnp.mean(tokens * tokens, axis=-1, keepdims=True) + NORM_EPS)
    normed = (tokens * scale * gain_ref[...]).astype(BF16)
    places = slots_of(route_ref[...], core_ref[0], experts)
    for block, send_ref in enumerate(send_refs):
        rows = send_ref.shape[0]
        number = lax.broadcasted_iota(jnp.int32, (rows, tokens.shape[0]), 0) + block * rows
        chosen = sum((b * rows + p == number).astype(F32) for b, p in places)
        send_ref[...] = mm(chosen.astype(BF16), normed, 1, 0).astype(BF16)


def dispatch(core, tokens, gain, routes, experts):
    rows = experts // 2 * TILE
    return pl.pallas_call(
        functools.partial(dispatch_kernel, experts),
        in_specs=[SMEM, VMEM, VMEM, VMEM],
        out_specs=[VMEM] * 4,
        out_shape=[jax.ShapeDtypeStruct((rows, tokens.shape[1]), BF16)] * 4,
        cost_estimate=pl.CostEstimate(
            flops=8 * tokens.size * rows, bytes_accessed=10 * tokens.size, transcendentals=0
        ),
        name="dispatch_rows",
    )(core, tokens, gain.reshape(1, -1), routes)


def combine_kernel(experts, first, core_ref, weight_ref, route_ref, *refs):
    back_refs, out_ref = refs[:-1], refs[-1]
    if first:
        base_ref, back_refs = back_refs[0], back_refs[1:]
    weights = weight_ref[...]
    tokens = weights.shape[1]
    places = slots_of(route_ref[...], core_ref[0], experts)
    total = base_ref[...] if first else 0.0
    for block, ref in enumerate(back_refs, first):
        rows = ref.shape[0]
        number = lax.broadcasted_iota(jnp.int32, (rows, tokens), 0) + block * rows
        mixed = sum(
            jnp.where(b * rows + p == number, weights[k : k + 1, :], 0.0)
            for k, (b, p) in enumerate(places)
        )
        high = mixed.astype(BF16)
        low = (mixed - high.astype(F32)).astype(BF16)
        total = total + (mm(high, ref[...], 0, 0) + mm(low, ref[...], 0, 0))
    out_ref[...] = total.astype(out_ref.dtype)


def combine(core, weights, routes, experts, returned, first=0, base=()):
    tokens = routes.shape[1]
    rows, features = returned[0].shape
    return pl.pallas_call(
        functools.partial(combine_kernel, experts, first),
        in_specs=[SMEM] + [VMEM] * (2 + len(base) + len(returned)),
        out_specs=VMEM,
        out_shape=jax.ShapeDtypeStruct((tokens, features), BF16 if first else F32),
        cost_estimate=pl.CostEstimate(
            flops=16 * tokens * rows * features, bytes_accessed=10 * rows * features, transcendentals=0
        ),
        name="combine_rows",
    )(core, weights, routes, *base, *returned)


def clamped_unit(gate_pre, up_pre):
    gate_pre = jnp.minimum(gate_pre, CLAMP_LIMIT)
    up_pre = jnp.clip(up_pre, -CLAMP_LIMIT, CLAMP_LIMIT)
    return (up_pre + 1.0) * gate_pre * jax.nn.sigmoid(SIGMOID_SCALE * gate_pre)


def expert_kernel(pieces, me_ref, gate_ref, up_ref, down_ref, *refs):
    row_refs, out_refs, rows_ref, total_ref = refs[:pieces], refs[pieces:-2], refs[-2], refs[-1]
    step = pl.program_id(0)

    @pl.when(step == 0)
    def _():
        start = 0
        for ref in row_refs:
            rows_ref[start : start + ref.shape[0], :] = ref[...]
            start += ref.shape[0]
        total_ref[...] = jnp.zeros_like(total_ref)

    rows = rows_ref[...]
    gate_pre = mm(rows, gate_ref[...], 1, 0)
    up_pre = mm(rows, up_ref[...], 1, 0)
    hidden = clamped_unit(gate_pre, up_pre).astype(BF16)
    total_ref[...] += mm(hidden, down_ref[...], 1, 0)

    @pl.when(step == pl.num_programs(0) - 1)
    def _():
        if len(out_refs) > 1:
            start = 0
            for ref in out_refs:
                ref[...] = total_ref[start : start + ref.shape[0], :].astype(BF16)
                start += ref.shape[0]
        else:
            (ref,) = out_refs
            owners, per = ref.shape[0], ref.shape[1]
            for k, by in enumerate((0, owners - 1, 1, 2)):
                owner = lax.rem(me_ref[0] + by, owners)
                ref[owner] = total_ref[k * per : (k + 1) * per, :].astype(BF16)


def expert_parts(me, pieces, gate_weight, up_weight, down_weight, owners=None):
    features, hidden = gate_weight.shape
    width = min(256, hidden)
    rows = sum(p.shape[0] for p in pieces)
    whole = [pl.BlockSpec(p.shape, lambda f: (0, 0)) for p in pieces]
    out_specs, out_shape = whole, [jax.ShapeDtypeStruct(p.shape, BF16) for p in pieces]
    if owners:
        by_owner = (owners, rows // owners, features)
        out_specs = [pl.BlockSpec(by_owner, lambda f: (0, 0, 0))]
        out_shape = [jax.ShapeDtypeStruct(by_owner, BF16)]
    return pl.pallas_call(
        functools.partial(expert_kernel, len(pieces)),
        grid=(hidden // width,),
        in_specs=[
            SMEM,
            pl.BlockSpec((features, width), lambda f: (0, f)),
            pl.BlockSpec((features, width), lambda f: (0, f)),
            pl.BlockSpec((width, features), lambda f: (f, 0)),
            *whole,
        ],
        out_specs=out_specs,
        out_shape=out_shape,
        scratch_shapes=[pltpu.VMEM((rows, features), BF16), pltpu.VMEM((rows, features), F32)],
        cost_estimate=pl.CostEstimate(
            flops=6 * rows * features * hidden,
            bytes_accessed=6 * features * hidden + 4 * rows * features,
            transcendentals=0,
        ),
        name="expert_parts",
    )(me, gate_weight, up_weight, down_weight, *pieces)


def turned(x, axis, by):
    size = lax.axis_size(axis)
    return lax.ppermute(x, axis, [(i, (i + by) % size) for i in range(size)])


def gathered_pieces(own):
    half = own.shape[0] // 2
    left = turned(own, "tp", 1)
    right = turned(own, "tp", -1)
    far_low = turned(left[:half], "tp", 1)
    far_high = turned(right[half:], "tp", -1)
    return own, left, right, far_low, far_high


def summed_pieces(parts):
    own, left, right, far_low, far_high = parts
    half = own.shape[0] // 2
    from_right = turned(far_low, "tp", -1)
    from_left = turned(far_high, "tp", 1)
    low = (left[:half].astype(F32) + from_right.astype(F32)).astype(BF16)
    high = (right[half:].astype(F32) + from_left.astype(F32)).astype(BF16)
    to_left = jnp.concatenate([low, left[half:]], axis=0)
    to_right = jnp.concatenate([right[:half], high], axis=0)
    back_right = turned(to_left, "tp", -1)
    back_left = turned(to_right, "tp", 1)
    return (own.astype(F32) + back_left.astype(F32) + back_right.astype(F32)).astype(BF16)


def sent_over_chips(rows, chips):
    blocks = rows.reshape(chips, -1, rows.shape[1])
    return lax.all_to_all(blocks, "ep_0", split_axis=0, concat_axis=0, tiled=True).reshape(rows.shape)


def after(value, earlier):
    return lax.optimization_barrier((value, earlier))[0]


def body(
    query,
    forget_gate_logits,
    value,
    forget_lower_margin,
    position_log_decay,
    head_norm_gain,
    mixer_output_weight,
    second_batch_tokens,
    expert_norm_gain,
    routes,
    chosen_expert_weight,
    gate_weight,
    up_weight,
    down_weight,
):
    n_ep = lax.axis_size(EP)
    chips = lax.axis_size("ep_0")
    owners = lax.axis_size("tp")
    core = lax.axis_index("ep_1").astype(jnp.int32).reshape(1)
    chip = lax.axis_index("ep_0").astype(jnp.int32).reshape(1)
    me = lax.axis_index("tp").astype(jnp.int32).reshape(1)
    place = jnp.stack([core[0], lax.axis_index("tp").astype(jnp.int32)])

    half = mixer_output_weight.shape[0] // 2
    weight_part = lax.dynamic_slice_in_dim(mixer_output_weight, core[0] * half, half, 0)
    weight_mine = lax.all_gather(weight_part, "tp", axis=0, tiled=False)
    weight_other = turned(weight_mine, "ep_1", 1)

    routes_t, weights_t = jnp.transpose(routes), jnp.transpose(chosen_expert_weight)
    near, far, late_near, late_far = dispatch(
        core, after(second_batch_tokens, weight_part), expert_norm_gain, routes_t, n_ep
    )
    far = turned(far, "ep_1", 1)
    late = late_near + turned(late_far, "ep_1", 1)

    state = mixer_states(
        forget_gate_logits, value, forget_lower_margin, position_log_decay
    )
    partner = turned(state, "ep_1", 1)
    chip_state = merged_states(core, state, partner)
    gathered = lax.all_gather(chip_state, "ep_0", axis=0, tiled=False)

    sums = []
    arrived = None
    for c, rows in enumerate((near, far, late)):
        if arrived is not None:
            rows = after(rows, (arrived, late))
        arrived = sent_over_chips(rows, chips)
        pieces = gathered_pieces(arrived)
        if not c:
            pieces = after(pieces, weight_mine)
        parts = expert_parts(
            me,
            pieces,
            gate_weight[0],
            up_weight[0],
            down_weight[0],
            owners if c else None,
        )
        if c:
            parts = parts[0].reshape(owners * rows.shape[0], -1)
            sums.append(lax.psum_scatter(parts, "tp", scatter_dimension=0, tiled=True))
        else:
            sums.append(summed_pieces(parts))

    returned = []
    for rows in sums:
        rows = after(rows, returned[-1] if returned else arrived)
        returned.append(sent_over_chips(rows, chips))

    entering_mine = entering_states(chip, gathered)
    entering_other = turned(entering_mine, "ep_1", 1)
    heads = mixer_heads(
        place,
        query,
        forget_gate_logits,
        value,
        forget_lower_margin,
        position_log_decay,
        head_norm_gain,
        entering_mine,
        entering_other,
        partner,
        owners,
    )
    heads = (
        heads[0],
        turned(heads[1], "tp", 1),
        turned(heads[owners - 1], "tp", -1),
        turned(heads[2], "tp", 2),
    )
    first_mixer_output = project(place, heads, weight_mine, weight_other)

    back_near, back_far, back_late = returned
    base = combine(core, weights_t, routes_t, n_ep, (back_near, turned(back_far, "ep_1", 1)))
    moe_out = combine(
        core,
        weights_t,
        routes_t,
        n_ep,
        (back_late, turned(back_late, "ep_1", 1)),
        2,
        (base,),
    )
    return (first_mixer_output, moe_out)


def solution(mesh):
    cores = 2
    finer = Mesh(
        mesh.devices.reshape(mesh.shape["grp"], mesh.shape["ep"] // cores, cores, mesh.shape["tp"]),
        ("grp", "ep_0", "ep_1", "tp"),
    )
    placed = (
        P(GRP_EP, "tp"),
        P(GRP_EP, "tp"),
        P(GRP_EP, "tp"),
        P(None, "tp"),
        P("tp", GRP_EP),
        P(),
        P("tp", None),
        P(GRP_EP_TP, None),
        P(),
        P(GRP_EP_TP, None),
        P(GRP_EP_TP, None),
        P(EP, None, "tp"),
        P(EP, None, "tp"),
        P(EP, "tp", None),
    )
    return jax.shard_map(
        body,
        mesh=finer,
        in_specs=placed,
        out_specs=(P(GRP_EP_TP, None), P(GRP_EP_TP, None)),
        check_vma=False,
    )
```

profile of v0, /device:TPU:33, one launch (start us, length us, event | category | flops | bytes accessed | tf_op | source)
XLA Modules:
  0.0 421.3 jit_solution(8519682915638246983)
XLA Ops:
  8.1 1.2 copy-done
  9.3 0.8 constant_dynamic-slice_fusion
  10.1 2.8 dispatch_rows.1
  13.0 24.5 %all-to-all-start = ((bf16[16,8,2048]{2,1,0:T(8,128)(2,1)}), bf16[16,8,2048]{2,1,0:T(8,128)(2,1)S(1)}, u32[]{:S(2)}, u32[]{:S(2)}) async-start(bf16[16,8,2048]{2,1,0:T(8,128)(2,1)} %bitcast.52), calls=%async_computation | async-start | bytes 1048576 | tf_op jit(solution)/shard_map/all_to_all | solution.py:483
  37.6 1.0 collective-permute-start.14
  38.8 1.5 collective-permute-done.14
  40.3 2.0 add.27
  42.3 18.0 %all-to-all-done = bf16[16,8,2048]{2,1,0:T(8,128)(2,1)S(1)} async-done(((bf16[16,8,2048]{2,1,0:T(8,128)(2,1)}), bf16[16,8,2048]{2,1,0:T(8,128)(2,1)S(1)}, u32[]{:S(2)}, u32[]{:S(2)}) %all-to-all-start) | async-done | bytes 524320 | tf_op jit(solution)/shard_map/all_to_all | solution.py:483
  60.2 35.3 %all_to_all.30 = bf16[16,8,2048]{2,1,0:T(8,128)(2,1)S(1)} all-to-all(bf16[16,8,2048]{2,1,0:T(8,128)(2,1)S(1)} %bitcast.53), channel_id=1, replica_groups=mesh['grp'=2,'ep_0'=16,'ep_1'=2,'tp'=4] {'ep_0'}, dimensions={0} | all-to-all | bytes 1048576 | tf_op jit(solution)/shard_map/all_to_all | solution.py:483
  95.5 1.3 collective-permute-start.16
  96.8 1.5 collective-permute-start.17
  98.4 6.6 %collective-permute-done.16.refs_1_ = bf16[128,2048]{1,0:T(8,128)(2,1)S(1)} collective-permute-done((bf16[128,2048]{1,0:T(8,128)(2,1)S(1)}, bf16[128,2048]{1,0:T(8,128)(2,1)S(1)}, u32[]{:S(2)}, u32[]{:S(2)}) %collective-permute-start.16) | collective-permute-done | bytes 524320 | tf_op jit(solution)/shard_map/ppermute | solution.py:455
  105.1 0.8 copy-done.16
  106.0 2.7 collective-permute-start.19
  108.7 5.9 %collective-permute-done.18.refs_3_ = bf16[64,2048]{1,0:T(8,128)(2,1)S(1)} collective-permute-done((bf16[64,2048]{1,0:T(8,128)(2,1)S(1)}, bf16[64,2048]{1,0:T(8,128)(2,1)S(1)}, u32[]{:S(2)}, u32[]{:S(2)}) %collective-permute-start.18) | collective-permute-done | bytes 262176 | tf_op jit(solution)/shard_map/ppermute | solution.py:455
  115.3 8.4 %expert_parts.4 = bf16[4,128,2048]{2,1,0:T(8,128)(2,1)} custom-call(s32[1]{0:T(128)} %bitcast.1.me_ref, bf16[2048,512]{1,0:T(8,128)(2,1)} %bitcast.59, bf16[2048,512]{1,0:T(8,128)(2,1)} %bitcast.62, bf16[512,2048]{1,0:T(8,128)(2,1)} %bitcast.65, bf16[128,2048]{1,0:T(8,128)(2,1)} %bitcast.51, bf16[128,2048]{1,0:T(8,128)(2,1)} %copy-done.15, ...), custom_call_target="tpu_custom_call" | custom-call | flops 3221225472 | bytes 10485760 | tf_op jit(solution)/shard_map/expert_parts/pallas_call | solution.py:431
  123.8 16.2 %all-to-all-start.2 = ((bf16[16,8,2048]{2,1,0:T(8,128)(2,1)}), bf16[16,8,2048]{2,1,0:T(8,128)(2,1)S(1)}, u32[]{:S(2)}, u32[]{:S(2)}) async-start(bf16[16,8,2048]{2,1,0:T(8,128)(2,1)} %bitcast.20), calls=%async_computation.2 | async-start | bytes 1048576 | tf_op jit(solution)/shard_map/all_to_all | solution.py:483
  140.2 2.9 collective-permute-start.7
  143.1 12.2 %collective-permute-done.6.refs_1_ = bf16[128,2048]{1,0:T(8,128)(2,1)S(1)} collective-permute-done((bf16[128,2048]{1,0:T(8,128)(2,1)S(1)}, bf16[128,2048]{1,0:T(8,128)(2,1)S(1)}, u32[]{:S(2)}, u32[]{:S(2)}) %collective-permute-start.6) | collective-permute-done | bytes 524320 | tf_op jit(solution)/shard_map/ppermute | solution.py:455
  155.7 0.8 collective-permute-done.7.refs_2_
  156.5 3.6 collective-permute-start.9
  160.2 9.3 %collective-permute-done.8.refs_3_ = bf16[64,2048]{1,0:T(8,128)(2,1)S(1)} collective-permute-done((bf16[64,2048]{1,0:T(8,128)(2,1)S(1)}, bf16[64,2048]{1,0:T(8,128)(2,1)S(1)}, u32[]{:S(2)}, u32[]{:S(2)}) %collective-permute-start.8) | collective-permute-done | bytes 262176 | tf_op jit(solution)/shard_map/ppermute | solution.py:455
  169.5 1.3 collective-permute-done.9.refs_4_
  170.8 0.7 copy-done.20
  171.5 8.4 %expert_parts.3 = (bf16[128,2048]{1,0:T(8,128)(2,1)}, bf16[128,2048]{1,0:T(8,128)(2,1)}, bf16[128,2048]{1,0:T(8,128)(2,1)}, bf16[64,2048]{1,0:T(8,128)(2,1)}, bf16[64,2048]{1,0:T(8,128)(2,1)}) custom-call(s32[1]{0:T(128)} %bitcast.1.me_ref, bf16[2048,512]{1,0:T(8,128)(2,1)} %bitcast.60, bf16[2048,512]{1,0:T(8,128)(2,1)} %bitcast.63, ...), custom_call_target="tpu_custom_call" | custom-call | flops 3221225472 | bytes 10485760 | tf_op jit(solution)/shard_map/expert_parts/pallas_call | solution.py:431
  179.9 3.6 collective-permute-start.12
  183.5 1.0 slice.51
  184.6 1.0 slice.48
  185.7 2.8 collective-permute-start.22
  188.5 1.0 add_convert_fusion.1
  189.5 1.7 collective-permute-start.13
  191.3 6.8 %collective-permute-done.21.refs_1_ = bf16[128,2048]{1,0:T(8,128)(2,1)S(1)} collective-permute-done((bf16[128,2048]{1,0:T(8,128)(2,1)S(1)}, bf16[128,2048]{1,0:T(8,128)(2,1)S(1)}, u32[]{:S(2)}, u32[]{:S(2)}) %collective-permute-start.21) | collective-permute-done | bytes 524320 | tf_op jit(solution)/shard_map/ppermute | solution.py:455
  198.9 2.4 collective-permute-start.24
  201.3 1.0 add_convert_fusion.2
  202.5 5.3 %collective-permute-done.23.refs_3_ = bf16[64,2048]{1,0:T(8,128)(2,1)S(1)} collective-permute-done((bf16[64,2048]{1,0:T(8,128)(2,1)S(1)}, bf16[64,2048]{1,0:T(8,128)(2,1)S(1)}, u32[]{:S(2)}, u32[]{:S(2)}) %collective-permute-start.23) | collective-permute-done | bytes 262176 | tf_op jit(solution)/shard_map/ppermute | solution.py:455
  207.7 0.7 copy-done.17
  208.4 6.1 %collective-permute-done.24.refs_4_ = bf16[64,2048]{1,0:T(8,128)(2,1)} collective-permute-done((bf16[64,2048]{1,0:T(8,128)(2,1)S(1)}, bf16[64,2048]{1,0:T(8,128)(2,1)}, u32[]{:S(2)}, u32[]{:S(2)}) %collective-permute-start.24) | collective-permute-done | bytes 262176 | tf_op jit(solution)/shard_map/ppermute | solution.py:455
  214.6 8.4 %expert_parts.5 = bf16[4,128,2048]{2,1,0:T(8,128)(2,1)} custom-call(s32[1]{0:T(128)} %bitcast.1.me_ref, bf16[2048,512]{1,0:T(8,128)(2,1)} %bitcast.61, bf16[2048,512]{1,0:T(8,128)(2,1)} %bitcast.64, bf16[512,2048]{1,0:T(8,128)(2,1)} %bitcast.67, bf16[128,2048]{1,0:T(8,128)(2,1)} %bitcast.47, bf16[128,2048]{1,0:T(8,128)(2,1)} %copy-done.11, ...), custom_call_target="tpu_custom_call" | custom-call | flops 3221225472 | bytes 10485760 | tf_op jit(solution)/shard_map/expert_parts/pallas_call | solution.py:431
  223.1 1.0 copy-done.6
  224.0 1.3 add_convert_fusion
  225.3 28.8 %all_to_all.31 = bf16[16,8,2048]{2,1,0:T(8,128)(2,1)} all-to-all(bf16[16,8,2048]{2,1,0:T(8,128)(2,1)S(1)} %bitcast.39), channel_id=1, replica_groups=mesh['grp'=2,'ep_0'=16,'ep_1'=2,'tp'=4] {'ep_0'}, dimensions={0} | all-to-all | bytes 1048576 | tf_op jit(solution)/shard_map/all_to_all | solution.py:483
  254.1 13.6 %all-to-all-start.4 = ((bf16[16,8,2048]{2,1,0:T(8,128)(2,1)}), bf16[16,8,2048]{2,1,0:T(8,128)(2,1)}, u32[]{:S(2)}, u32[]{:S(2)}) async-start(bf16[16,8,2048]{2,1,0:T(8,128)(2,1)} %bitcast.41), calls=%async_computation.5 | async-start | bytes 1048576 | tf_op jit(solution)/shard_map/all_to_all | solution.py:483
  267.7 10.4 %mixer_states.1.own_ref = bf16[2,2,144,128]{3,2,1,0:T(8,128)(2,1)} custom-call(bf16[1024,256]{1,0:T(8,128)(2,1)} %logits_ref.3, bf16[1024,256]{1,0:T(8,128)(2,1)} %value_ref.3, f32[2,256]{1,0:T(2,128)} %margin_ref.3, f32[2,1024]{1,0:T(2,128)} %decay_ref.3), custom_call_target="tpu_custom_call" | custom-call | flops 805306368 | bytes 1310720 | tf_op jit(solution)/shard_map/mixer_states/pallas_call | solution.py:107
  278.1 4.0 collective-permute-start
  282.2 1.2 collective-permute-done.partner_ref
  283.4 0.7 copy-done.7
  284.0 1.7 mixer_merge.1
  285.8 4.2 all-to-all-done.4
  289.9 11.9 %all-to-all-start.5 = ((bf16[16,8,2048]{2,1,0:T(8,128)(2,1)}), bf16[16,8,2048]{2,1,0:T(8,128)(2,1)}, u32[]{:S(2)}, u32[]{:S(2)}) async-start(bf16[16,8,2048]{2,1,0:T(8,128)(2,1)} %bitcast.48), calls=%async_computation.7 | async-start | bytes 1048576 | tf_op jit(solution)/shard_map/all_to_all | solution.py:483
  301.8 2.4 collective-permute-start.5
  304.3 56.9 %all-gather.5.cloned.1.call-done = bf16[32,144,128]{2,1,0:T(8,128)(2,1)} async-done(((bf16[2,144,128]{2,1,0:T(8,128)(2,1)}), bf16[32,144,128]{2,1,0:T(8,128)(2,1)}) %all-gather.5.cloned.1.call-update) | async-done | bytes 1179664 | tf_op jit(solution)/shard_map/all_gather | solution.py:531
  361.2 2.6 mixer_entering.1.mine_ref
  363.8 7.6 %collective-permute-start.1 = (bf16[2,128,128]{2,1,0:T(8,128)(2,1)}, bf16[2,128,128]{2,1,0:T(8,128)(2,1)S(1)}, u32[]{:S(2)}, u32[]{:S(2)}) collective-permute-start(bf16[2,128,128]{2,1,0:T(8,128)(2,1)} %mixer_entering.1.mine_ref), channel_id=1, source_target_pairs={{0,4},{4,0},{1,5},{5,1},{2,6},{6,2},{3,7},{7,3},{8,12},{12,8},{9,1... | collective-permute-start | bytes 196616 | tf_op jit(solution)/shard_map/ppermute | solution.py:455
  373.1 13.2 %mixer_heads.1 = bf16[4,2,256,128]{3,2,1,0:T(8,128)(2,1)} custom-call(s32[2]{0:T(128)} %pad_add_fusion.place_ref, bf16[1024,256]{1,0:T(8,128)(2,1)} %query_ref.1, bf16[1024,256]{1,0:T(8,128)(2,1)} %logits_ref.3, bf16[1024,256]{1,0:T(8,128)(2,1)} %value_ref.3, f32[2,256]{1,0:T(2,128)} %margin_ref.3, f32[2,1024]{1,0:T(2,128)} %decay_ref.3, f32[1,128]{1,0:T(1,128)} %bitcast.69, ...), custom_call_target="tpu_custom_call" | custom-call | flops 1610612736 | bytes 4194304 | tf_op jit(solution)/shard_map/mixer_heads/pallas_call | solution.py:255
  386.8 1.8 slice_bitcast_fusion
  388.5 1.1 collective-permute-start.2
  389.7 1.7 collective-permute-start.3
  391.4 3.4 collective-permute-done.2.left_ref
  394.8 0.8 collective-permute-start.4
  395.7 4.5 %collective-permute-done.4.far_ref = bf16[2,256,128]{2,1,0:T(8,128)(2,1)S(1)} collective-permute-done((bf16[2,256,128]{2,1,0:T(8,128)(2,1)S(1)}, bf16[2,256,128]{2,1,0:T(8,128)(2,1)S(1)}, u32[]{:S(2)}, u32[]{:S(2)}) %collective-permute-start.4) | collective-permute-done | bytes 131104 | tf_op jit(solution)/shard_map/ppermute | solution.py:455
  400.2 0.6 copy-done.10
  400.8 6.9 %mixer_project.1 = bf16[256,2048]{1,0:T(8,128)(2,1)} custom-call(s32[2]{0:T(128)} %pad_add_fusion.place_ref, bf16[2,256,128]{2,1,0:T(8,128)(2,1)} %get-tuple-element.45.own_ref, bf16[2,256,128]{2,1,0:T(8,128)(2,1)} %copy-done.8, bf16[2,256,128]{2,1,0:T(8,128)(2,1)} %copy-done.9, bf16[2,256,128]{2,1,0:T(8,128)(2,1)} %copy-done.10, ...), custom_call_target="tpu_custom_call" | custom-call | flops 1073741824 | bytes 4194304 | tf_op jit(solution)/shard_map/mixer_project/pallas_call | solution.py:288
  407.8 3.2 combine_rows.2.refs_0_
  410.9 3.2 combine_rows.3
  (82 shorter events, 5.6 us)
Async XLA Ops:
  8.0 1.2 copy-start
  13.0 47.3 %all-to-all-start = ((bf16[16,8,2048]{2,1,0:T(8,128)(2,1)}), bf16[16,8,2048]{2,1,0:T(8,128)(2,1)S(1)}, u32[]{:S(2)}, u32[]{:S(2)}) async-start(bf16[16,8,2048]{2,1,0:T(8,128)(2,1)} %bitcast.52), calls=%async_computation | async-start | bytes 1048576 | tf_op jit(solution)/shard_map/all_to_all | solution.py:483
  37.5 133.3 %all-gather.7.cloned.1.call-start = ((), (), s32[]{:S(2)}) async-start(), calls=%async_computation.11 | async-start | bytes 2621440 | tf_op jit(solution)/shard_map/all_gather | solution.py:516
  37.6 2.8 collective-permute-start.14
  38.6 3.7 collective-permute-start.15
  38.8 215.3 %reduce-scatter.3.cloned.1.call-start = ((), (), s32[]{:S(2)}) async-start(), calls=%async_computation.8 | async-start | bytes 2621440 | tf_op jit(solution)/shard_map/reduce_scatter | solution.py:552
  60.2 80.0 %copy-start.3 = (bf16[16,8,2048]{2,1,0:T(8,128)(2,1)}, bf16[16,8,2048]{2,1,0:T(8,128)(2,1)S(1)}, u32[]{:S(2)}) copy-start(bf16[16,8,2048]{2,1,0:T(8,128)(2,1)S(1)} %all-to-all-done) | copy-start | bytes 1572868
  95.5 19.3 %copy-start.5 = (bf16[16,8,2048]{2,1,0:T(8,128)(2,1)}, bf16[16,8,2048]{2,1,0:T(8,128)(2,1)S(1)}, u32[]{:S(2)}) copy-start(bf16[16,8,2048]{2,1,0:T(8,128)(2,1)S(1)} %all_to_all.30) | copy-start | bytes 1572868
  95.5 9.5 %collective-permute-start.16 = (bf16[128,2048]{1,0:T(8,128)(2,1)S(1)}, bf16[128,2048]{1,0:T(8,128)(2,1)S(1)}, u32[]{:S(2)}, u32[]{:S(2)}) collective-permute-start(bf16[128,2048]{1,0:T(8,128)(2,1)S(1)} %bitcast.49), channel_id=1, source_target_pairs={{0,1},{1,2},{2,3},{3,0},{4,5},{5,6},{6,7},{7,4},{8,9},{9,10},{10,1... | collective-permute-start | bytes 1572872 | tf_op jit(solution)/shard_map/ppermute | solution.py:455
  96.8 8.3 %collective-permute-start.17 = (bf16[128,2048]{1,0:T(8,128)(2,1)S(1)}, bf16[128,2048]{1,0:T(8,128)(2,1)S(1)}, u32[]{:S(2)}, u32[]{:S(2)}) collective-permute-start(bf16[128,2048]{1,0:T(8,128)(2,1)S(1)} %bitcast.50), channel_id=1, source_target_pairs={{0,3},{1,0},{2,1},{3,2},{4,7},{5,4},{6,5},{7,6},{8,11},{9,8},{10,9... | collective-permute-start | bytes 1572872 | tf_op jit(solution)/shard_map/ppermute | solution.py:455
  105.0 9.9 %copy-start.15 = (bf16[128,2048]{1,0:T(8,128)(2,1)}, bf16[128,2048]{1,0:T(8,128)(2,1)S(1)}, u32[]{:S(2)}) copy-start(bf16[128,2048]{1,0:T(8,128)(2,1)S(1)} %collective-permute-done.16.refs_1_) | copy-start | bytes 1572868
  105.0 9.6 %collective-permute-start.18 = (bf16[64,2048]{1,0:T(8,128)(2,1)S(1)}, bf16[64,2048]{1,0:T(8,128)(2,1)S(1)}, u32[]{:S(2)}, u32[]{:S(2)}) collective-permute-start(bf16[64,2048]{1,0:T(8,128)(2,1)S(1)} %slice.62), channel_id=1, source_target_pairs={{0,1},{1,2},{2,3},{3,0},{4,5},{5,6},{6,7},{7,4},{8,9},{9,10},{10,1... | collective-permute-start | bytes 786440 | tf_op jit(solution)/shard_map/ppermute | solution.py:455
  105.1 0.8 copy-start.16
  106.0 8.9 %collective-permute-start.19 = (bf16[64,2048]{1,0:T(8,128)(2,1)S(1)}, bf16[64,2048]{1,0:T(8,128)(2,1)}, u32[]{:S(2)}, u32[]{:S(2)}) collective-permute-start(bf16[64,2048]{1,0:T(8,128)(2,1)S(1)} %slice.63), channel_id=1, source_target_pairs={{0,3},{1,0},{2,1},{3,2},{4,7},{5,4},{6,5},{7,6},{8,11},{9,8},{10,9... | collective-permute-start | bytes 786440 | tf_op jit(solution)/shard_map/ppermute | solution.py:455
  114.6 0.7 copy-start.19
  123.8 61.8 %all-to-all-start.2 = ((bf16[16,8,2048]{2,1,0:T(8,128)(2,1)}), bf16[16,8,2048]{2,1,0:T(8,128)(2,1)S(1)}, u32[]{:S(2)}, u32[]{:S(2)}) async-start(bf16[16,8,2048]{2,1,0:T(8,128)(2,1)} %bitcast.20), calls=%async_computation.2 | async-start | bytes 1048576 | tf_op jit(solution)/shard_map/all_to_all | solution.py:483
  140.0 149.9 %reduce-scatter.5.cloned.1.call-start = ((), (), s32[]{:S(2)}) async-start(), calls=%async_computation.9 | async-start | bytes 2621440 | tf_op jit(solution)/shard_map/reduce_scatter | solution.py:552
  140.1 15.3 %collective-permute-start.6 = (bf16[128,2048]{1,0:T(8,128)(2,1)S(1)}, bf16[128,2048]{1,0:T(8,128)(2,1)S(1)}, u32[]{:S(2)}, u32[]{:S(2)}) collective-permute-start(bf16[128,2048]{1,0:T(8,128)(2,1)S(1)} %bitcast.42), channel_id=1, source_target_pairs={{0,1},{1,2},{2,3},{3,0},{4,5},{5,6},{6,7},{7,4},{8,9},{9,10},{10,1... | collective-permute-start | bytes 1572872 | tf_op jit(solution)/shard_map/ppermute | solution.py:455
  140.2 16.3 %collective-permute-start.7 = (bf16[128,2048]{1,0:T(8,128)(2,1)S(1)}, bf16[128,2048]{1,0:T(8,128)(2,1)S(1)}, u32[]{:S(2)}, u32[]{:S(2)}) collective-permute-start(bf16[128,2048]{1,0:T(8,128)(2,1)S(1)} %bitcast.43), channel_id=1, source_target_pairs={{0,3},{1,0},{2,1},{3,2},{4,7},{5,4},{6,5},{7,6},{8,11},{9,8},{10,9... | collective-permute-start | bytes 1572872 | tf_op jit(solution)/shard_map/ppermute | solution.py:455
  155.4 15.4 %copy-start.13 = (bf16[128,2048]{1,0:T(8,128)(2,1)}, bf16[128,2048]{1,0:T(8,128)(2,1)S(1)}, u32[]{:S(2)}) copy-start(bf16[128,2048]{1,0:T(8,128)(2,1)S(1)} %collective-permute-done.6.refs_1_) | copy-start | bytes 1572868
  155.4 14.1 %collective-permute-start.8 = (bf16[64,2048]{1,0:T(8,128)(2,1)S(1)}, bf16[64,2048]{1,0:T(8,128)(2,1)S(1)}, u32[]{:S(2)}, u32[]{:S(2)}) collective-permute-start(bf16[64,2048]{1,0:T(8,128)(2,1)S(1)} %slice.60), channel_id=1, source_target_pairs={{0,1},{1,2},{2,3},{3,0},{4,5},{5,6},{6,7},{7,4},{8,9},{9,10},{10,1... | collective-permute-start | bytes 786440 | tf_op jit(solution)/shard_map/ppermute | solution.py:455
  156.5 14.3 %copy-start.14 = (bf16[128,2048]{1,0:T(8,128)(2,1)}, bf16[128,2048]{1,0:T(8,128)(2,1)S(1)}, u32[]{:S(2)}) copy-start(bf16[128,2048]{1,0:T(8,128)(2,1)S(1)} %collective-permute-done.7.refs_2_) | copy-start | bytes 1572868
  156.5 14.2 %collective-permute-start.9 = (bf16[64,2048]{1,0:T(8,128)(2,1)S(1)}, bf16[64,2048]{1,0:T(8,128)(2,1)S(1)}, u32[]{:S(2)}, u32[]{:S(2)}) collective-permute-start(bf16[64,2048]{1,0:T(8,128)(2,1)S(1)} %slice.61), channel_id=1, source_target_pairs={{0,3},{1,0},{2,1},{3,2},{4,7},{5,4},{6,5},{7,6},{8,11},{9,8},{10,9... | collective-permute-start | bytes 786440 | tf_op jit(solution)/shard_map/ppermute | solution.py:455
  169.5 1.3 copy-start.18
  170.8 0.7 copy-start.20
  179.9 21.4 %copy-start.2 = (bf16[128,2048]{1,0:T(8,128)(2,1)S(1)}, bf16[128,2048]{1,0:T(8,128)(2,1)}, u32[]{:S(2)}) copy-start(bf16[128,2048]{1,0:T(8,128)(2,1)} %get-tuple-element.30) | copy-start | bytes 1572868
  179.9 8.6 %collective-permute-start.12 = (bf16[64,2048]{1,0:T(8,128)(2,1)}, bf16[64,2048]{1,0:T(8,128)(2,1)S(1)}, u32[]{:S(2)}, u32[]{:S(2)}) collective-permute-start(bf16[64,2048]{1,0:T(8,128)(2,1)} %get-tuple-element.33), channel_id=1, source_target_pairs={{0,3},{1,0},{2,1},{3,2},{4,7},{5,4},{6,5},{7,6},{8,11},{9,8},{10,9... | collective-permute-start | bytes 786440 | tf_op jit(solution)/shard_map/ppermute | solution.py:455
  184.4 16.8 %collective-permute-start.10 = (bf16[64,2048]{1,0:T(8,128)(2,1)}, bf16[64,2048]{1,0:T(8,128)(2,1)}, u32[]{:S(2)}, u32[]{:S(2)}) collective-permute-start(bf16[64,2048]{1,0:T(8,128)(2,1)} %get-tuple-element.31), channel_id=1, source_target_pairs={{0,1},{1,2},{2,3},{3,0},{4,5},{5,6},{6,7},{7,4},{8,9},{9,10},{10,1... | collective-permute-start | bytes 786440 | tf_op jit(solution)/shard_map/ppermute | solution.py:455
  185.6 16.8 %copy-start.4 = (bf16[16,8,2048]{2,1,0:T(8,128)(2,1)}, bf16[16,8,2048]{2,1,0:T(8,128)(2,1)S(1)}, u32[]{:S(2)}) copy-start(bf16[16,8,2048]{2,1,0:T(8,128)(2,1)S(1)} %all-to-all-done.2) | copy-start | bytes 1572868
  185.6 12.5 %collective-permute-start.21 = (bf16[128,2048]{1,0:T(8,128)(2,1)S(1)}, bf16[128,2048]{1,0:T(8,128)(2,1)S(1)}, u32[]{:S(2)}, u32[]{:S(2)}) collective-permute-start(bf16[128,2048]{1,0:T(8,128)(2,1)S(1)} %bitcast.45), channel_id=1, source_target_pairs={{0,1},{1,2},{2,3},{3,0},{4,5},{5,6},{6,7},{7,4},{8,9},{9,10},{10,1... | collective-permute-start | bytes 1572872 | tf_op jit(solution)/shard_map/ppermute | solution.py:455
  185.7 13.1 %collective-permute-start.22 = (bf16[128,2048]{1,0:T(8,128)(2,1)S(1)}, bf16[128,2048]{1,0:T(8,128)(2,1)S(1)}, u32[]{:S(2)}, u32[]{:S(2)}) collective-permute-start(bf16[128,2048]{1,0:T(8,128)(2,1)S(1)} %bitcast.46), channel_id=1, source_target_pairs={{0,3},{1,0},{2,1},{3,2},{4,7},{5,4},{6,5},{7,6},{8,11},{9,8},{10,9... | collective-permute-start | bytes 1572872 | tf_op jit(solution)/shard_map/ppermute | solution.py:455
  189.5 33.5 %collective-permute-start.13 = (bf16[128,2048]{1,0:T(8,128)(2,1)S(1)}, bf16[128,2048]{1,0:T(8,128)(2,1)S(1)}, u32[]{:S(2)}, u32[]{:S(2)}) collective-permute-start(bf16[128,2048]{1,0:T(8,128)(2,1)S(1)} %pad_maximum_fusion.1), channel_id=1, source_target_pairs={{0,3},{1,0},{2,1},{3,2},{4,7},{5,4},{6,5},{7,6},{8,11},{9,8},{10,9... | collective-permute-start | bytes 1572872 | tf_op jit(solution)/shard_map/ppermute | solution.py:455
  198.1 0.8 copy-start.11
  198.1 9.6 %collective-permute-start.23 = (bf16[64,2048]{1,0:T(8,128)(2,1)S(1)}, bf16[64,2048]{1,0:T(8,128)(2,1)S(1)}, u32[]{:S(2)}, u32[]{:S(2)}) collective-permute-start(bf16[64,2048]{1,0:T(8,128)(2,1)S(1)} %slice.64), channel_id=1, source_target_pairs={{0,1},{1,2},{2,3},{3,0},{4,5},{5,6},{6,7},{7,4},{8,9},{9,10},{10,1... | collective-permute-start | bytes 786440 | tf_op jit(solution)/shard_map/ppermute | solution.py:455
  198.8 8.9 %copy-start.12 = (bf16[128,2048]{1,0:T(8,128)(2,1)}, bf16[128,2048]{1,0:T(8,128)(2,1)S(1)}, u32[]{:S(2)}) copy-start(bf16[128,2048]{1,0:T(8,128)(2,1)S(1)} %collective-permute-done.22.refs_2_) | copy-start | bytes 1572868
  198.9 15.7 %collective-permute-start.24 = (bf16[64,2048]{1,0:T(8,128)(2,1)S(1)}, bf16[64,2048]{1,0:T(8,128)(2,1)}, u32[]{:S(2)}, u32[]{:S(2)}) collective-permute-start(bf16[64,2048]{1,0:T(8,128)(2,1)S(1)} %slice.65), channel_id=1, source_target_pairs={{0,3},{1,0},{2,1},{3,2},{4,7},{5,4},{6,5},{7,6},{8,11},{9,8},{10,9... | collective-permute-start | bytes 786440 | tf_op jit(solution)/shard_map/ppermute | solution.py:455
  202.3 20.7 %collective-permute-start.11 = (bf16[128,2048]{1,0:T(8,128)(2,1)S(1)}, bf16[128,2048]{1,0:T(8,128)(2,1)}, u32[]{:S(2)}, u32[]{:S(2)}) collective-permute-start(bf16[128,2048]{1,0:T(8,128)(2,1)S(1)} %pad_maximum_fusion), channel_id=1, source_target_pairs={{0,1},{1,2},{2,3},{3,0},{4,5},{5,6},{6,7},{7,4},{8,9},{9,10},{10,1... | collective-permute-start | bytes 1572872 | tf_op jit(solution)/shard_map/ppermute | solution.py:455
  207.7 0.7 copy-start.17
  223.0 1.0 copy-start.6
  254.1 35.9 %all-to-all-start.4 = ((bf16[16,8,2048]{2,1,0:T(8,128)(2,1)}), bf16[16,8,2048]{2,1,0:T(8,128)(2,1)}, u32[]{:S(2)}, u32[]{:S(2)}) async-start(bf16[16,8,2048]{2,1,0:T(8,128)(2,1)} %bitcast.41), calls=%async_computation.5 | async-start | bytes 1048576 | tf_op jit(solution)/shard_map/all_to_all | solution.py:483
  267.7 34.2 %copy-start.1 = (bf16[512,2048]{1,0:T(8,128)(2,1)S(1)}, bf16[512,2048]{1,0:T(8,128)(2,1)}, u32[]{:S(2)}) copy-start(bf16[512,2048]{1,0:T(8,128)(2,1)} %all-gather.7.cloned.1.call-done) | copy-start | bytes 6291460
  267.7 93.5 %all-gather.5.cloned.1.call-start = ((), (), s32[]{:S(2)}) async-start(), calls=%async_computation.10 | async-start | bytes 1253376 | tf_op jit(solution)/shard_map/all_gather | solution.py:531
  278.1 5.2 %collective-permute-start = (bf16[2,2,144,128]{3,2,1,0:T(8,128)(2,1)}, bf16[2,2,144,128]{3,2,1,0:T(8,128)(2,1)S(1)}, u32[]{:S(2)}, u32[]{:S(2)}) collective-permute-start(bf16[2,2,144,128]{3,2,1,0:T(8,128)(2,1)} %mixer_states.1.own_ref), channel_id=1, source_target_pairs={{0,4},{4,0},{1,5},{5,1},{2,6},{6,2},{3,7},{7,3},{8,12},{12,8},{9,1... | collective-permute-start | bytes 442376 | tf_op jit(solution)/shard_map/ppermute | solution.py:455
  283.4 0.7 copy-start.7
  289.9 96.7 %all-to-all-start.5 = ((bf16[16,8,2048]{2,1,0:T(8,128)(2,1)}), bf16[16,8,2048]{2,1,0:T(8,128)(2,1)}, u32[]{:S(2)}, u32[]{:S(2)}) async-start(bf16[16,8,2048]{2,1,0:T(8,128)(2,1)} %bitcast.48), calls=%async_computation.7 | async-start | bytes 1048576 | tf_op jit(solution)/shard_map/all_to_all | solution.py:483
  301.8 98.3 %collective-permute-start.5 = (bf16[4,128,2048]{2,1,0:T(8,128)(2,1)S(1)}, bf16[4,128,2048]{2,1,0:T(8,128)(2,1)}, u32[]{:S(2)}, u32[]{:S(2)}) collective-permute-start(bf16[4,128,2048]{2,1,0:T(8,128)(2,1)S(1)} %bitcast.35), channel_id=1, source_target_pairs={{0,4},{4,0},{1,5},{5,1},{2,6},{6,2},{3,7},{7,3},{8,12},{12,8},{9,1... | collective-permute-start | bytes 6291464 | tf_op jit(solution)/shard_map/ppermute | solution.py:455
  363.8 8.7 %collective-permute-start.1 = (bf16[2,128,128]{2,1,0:T(8,128)(2,1)}, bf16[2,128,128]{2,1,0:T(8,128)(2,1)S(1)}, u32[]{:S(2)}, u32[]{:S(2)}) collective-permute-start(bf16[2,128,128]{2,1,0:T(8,128)(2,1)} %mixer_entering.1.mine_ref), channel_id=1, source_target_pairs={{0,4},{4,0},{1,5},{5,1},{2,6},{6,2},{3,7},{7,3},{8,12},{12,8},{9,1... | collective-permute-start | bytes 196616 | tf_op jit(solution)/shard_map/ppermute | solution.py:455
  372.5 0.6 copy-start.21
  386.3 21.5 %collective-permute-start.20 = (bf16[128,2048]{1,0:T(8,128)(2,1)}, bf16[128,2048]{1,0:T(8,128)(2,1)}, u32[]{:S(2)}, u32[]{:S(2)}) collective-permute-start(bf16[128,2048]{1,0:T(8,128)(2,1)} %bitcast.26), channel_id=1, source_target_pairs={{0,4},{4,0},{1,5},{5,1},{2,6},{6,2},{3,7},{7,3},{8,12},{12,8},{9,1... | collective-permute-start | bytes 1572872 | tf_op jit(solution)/shard_map/ppermute | solution.py:455
  386.6 24.3 %collective-permute-start.25 = (bf16[128,2048]{1,0:T(8,128)(2,1)}, bf16[128,2048]{1,0:T(8,128)(2,1)}, u32[]{:S(2)}, u32[]{:S(2)}) collective-permute-start(bf16[128,2048]{1,0:T(8,128)(2,1)} %bitcast.29.refs_1_), channel_id=1, source_target_pairs={{0,4},{4,0},{1,5},{5,1},{2,6},{6,2},{3,7},{7,3},{8,12},{12,8},{9,1... | collective-permute-start | bytes 1572872 | tf_op jit(solution)/shard_map/ppermute | solution.py:455
  388.5 6.3 %collective-permute-start.2 = (bf16[2,256,128]{2,1,0:T(8,128)(2,1)S(1)}, bf16[2,256,128]{2,1,0:T(8,128)(2,1)S(1)}, u32[]{:S(2)}, u32[]{:S(2)}) collective-permute-start(bf16[2,256,128]{2,1,0:T(8,128)(2,1)S(1)} %get-tuple-element.44), channel_id=1, source_target_pairs={{0,1},{1,2},{2,3},{3,0},{4,5},{5,6},{6,7},{7,4},{8,9},{9,10},{10,1... | collective-permute-start | bytes 393224 | tf_op jit(solution)/shard_map/ppermute | solution.py:455
  389.7 6.0 %collective-permute-start.3 = (bf16[2,256,128]{2,1,0:T(8,128)(2,1)S(1)}, bf16[2,256,128]{2,1,0:T(8,128)(2,1)S(1)}, u32[]{:S(2)}, u32[]{:S(2)}) collective-permute-start(bf16[2,256,128]{2,1,0:T(8,128)(2,1)S(1)} %get-tuple-element.43), channel_id=1, source_target_pairs={{0,3},{1,0},{2,1},{3,2},{4,7},{5,4},{6,5},{7,6},{8,11},{9,8},{10,9... | collective-permute-start | bytes 393224 | tf_op jit(solution)/shard_map/ppermute | solution.py:455
  394.8 5.3 %copy-start.8 = (bf16[2,256,128]{2,1,0:T(8,128)(2,1)}, bf16[2,256,128]{2,1,0:T(8,128)(2,1)S(1)}, u32[]{:S(2)}) copy-start(bf16[2,256,128]{2,1,0:T(8,128)(2,1)S(1)} %collective-permute-done.2.left_ref) | copy-start | bytes 393220
  394.8 5.3 %collective-permute-start.4 = (bf16[2,256,128]{2,1,0:T(8,128)(2,1)S(1)}, bf16[2,256,128]{2,1,0:T(8,128)(2,1)S(1)}, u32[]{:S(2)}, u32[]{:S(2)}) collective-permute-start(bf16[2,256,128]{2,1,0:T(8,128)(2,1)S(1)} %get-tuple-element.42), channel_id=1, source_target_pairs={{0,2},{1,3},{2,0},{3,1},{4,6},{5,7},{6,4},{7,5},{8,10},{9,11},{10,... | collective-permute-start | bytes 393224 | tf_op jit(solution)/shard_map/ppermute | solution.py:455
  395.7 4.5 %copy-start.9 = (bf16[2,256,128]{2,1,0:T(8,128)(2,1)}, bf16[2,256,128]{2,1,0:T(8,128)(2,1)S(1)}, u32[]{:S(2)}) copy-start(bf16[2,256,128]{2,1,0:T(8,128)(2,1)S(1)} %collective-permute-done.3.right_ref) | copy-start | bytes 393220
  400.1 0.7 copy-start.10
Sparse Core Ops, SparseCore 0:
  40.7 38.7 all-gather.6
  123.9 54.5 reduce-scatter.2
  223.2 44.0 reduce-scatter.4
Sparse Core Ops, SparseCore 1:
  285.8 75.3 all-gather.4
where the time goes:
time: 424 us; the launch traced here: 421 us
  waiting for transfers between devices  145 us (34%)
  starting transfers between devices  110 us (26%)
  Pallas kernels  69.2 us (16%)
  blocking collectives  64 us (15%)
  between operations  15.5 us (4%)
  local copies, waits for them, and re-layouts  12.1 us (3%)
  other arithmetic  5.97 us (1%)
    all_to_all x4, starting transfers between devices, sent_over_chips(): lax.all_to_all(blocks, 'ep_0', split_axis=0, concat_axis=0, tiled=True)  66.3 us
    ppermute x26, waiting for transfers between devices, turned(): return lax.ppermute(x, axis, [(i, (i + by) % size) for i in range(size)])  65.5 us
    all_to_all x2, blocking collectives, sent_over_chips(): lax.all_to_all(blocks, 'ep_0', split_axis=0, concat_axis=0, tiled=True)  64 us
    all_gather x1, waiting for transfers between devices, body(): gathered = lax.all_gather(chip_state, 'ep_0', axis=0, tiled=False)  56.9 us
    ppermute x26, starting transfers between devices, turned(): return lax.ppermute(x, axis, [(i, (i + by) % size) for i in range(size)])  43.2 us
    pallas_call x3, Pallas kernels, expert_parts(): pl.pallas_call(functools.partial(expert_kernel, len(pieces)), grid=(hidde...  25.2 us
    all_to_all x4, waiting for transfers between devices, sent_over_chips(): lax.all_to_all(blocks, 'ep_0', split_axis=0, concat_axis=0, tiled=True)  22.1 us
    pallas_call x1, Pallas kernels, mixer_heads(): pl.pallas_call(heads_kernel, in_specs=[SMEM] + [VMEM] * 9, out_specs=VMEM...  13.2 us
  transfers between devices with their start and end apart: 34, of which 18 were waited for; matrix products, arithmetic and copies ran while one was open for 2% of the time, Pallas kernels for 15%

commit v1 on v0

--- a/solution.py
+++ b/solution.py
@@ -265,36 +265,37 @@
     )(place, query, logits, value, margin, decay, gain.reshape(1, HEAD_CHANNELS), mine, other, partner)
 
 
-def project_kernel(place_ref, own_ref, left_ref, right_ref, far_ref, mine_ref, other_ref, out_ref):
-    core, me = place_ref[0], place_ref[1]
-    owners = mine_ref.shape[0]
+def project_kernel(own_ref, left_ref, right_ref, far_ref, *refs):
+    own_w, left_w, right_w, far_low_w, far_high_w, out_ref = refs
     width = 256
 
     def columns(c, _):
         cols = pl.ds(pl.multiple_of(c * width, width), width)
         total = jnp.zeros((out_ref.shape[0], width), F32)
-        for ref, by in ((own_ref, 0), (left_ref, owners - 1), (right_ref, 1), (far_ref, 2)):
-            source = lax.rem(me + by, owners)
-            total += mm(ref[core], mine_ref[source, :, cols], 1, 0)
-            total += mm(ref[1 - core], other_ref[source, :, cols], 1, 0)
+        for h in range(own_ref.shape[0]):
+            rows = columns_of(h)
+            total += mm(own_ref[h], own_w[rows, cols], 1, 0)
+            total += mm(left_ref[h], left_w[rows, cols], 1, 0)
+            total += mm(right_ref[h], right_w[rows, cols], 1, 0)
+            total += mm(far_ref[h], (far_low_w, far_high_w)[h][:, cols], 1, 0)
         out_ref[:, cols] = total.astype(BF16)
         return 0
 
     lax.fori_loop(0, out_ref.shape[1] // width, columns, 0)
 
 
-def project(place, heads, mine, other):
-    tokens, features = heads[0].shape[1], mine.shape[2]
+def project(heads, weights):
+    tokens, features = heads[0].shape[1], weights[0].shape[1]
     return pl.pallas_call(
         project_kernel,
-        in_specs=[SMEM] + [VMEM] * 6,
+        in_specs=[VMEM] * 9,
         out_specs=VMEM,
         out_shape=jax.ShapeDtypeStruct((tokens, features), BF16),
         cost_estimate=pl.CostEstimate(
             flops=8 * heads[0].size * features, bytes_accessed=8 * tokens * features, transcendentals=0
         ),
         name="mixer_project",
-    )(place, *heads, mine, other)
+    )(*heads, *weights)
 
 
 def slots_of(routes, core, experts):
@@ -317,25 +318,38 @@
     return result
 
 
-def dispatch_kernel(experts, core_ref, token_ref, gain_ref, route_ref, *send_refs):
+def dispatch_kernel(experts, core_ref, token_ref, gain_ref, route_ref, *refs):
+    near_ref, others_ref, late_ref, normed_ref, chosen_ref = refs
     tokens = token_ref[...].astype(F32)
     scale = lax.rsqrt(jnp.mean(tokens * tokens, axis=-1, keepdims=True) + NORM_EPS)
-    normed = (tokens * scale * gain_ref[...]).astype(BF16)
+    normed_ref[...] = (tokens * scale * gain_ref[...]).astype(BF16)
+    rows = near_ref.shape[0]
     places = slots_of(route_ref[...], core_ref[0], experts)
-    for block, send_ref in enumerate(send_refs):
-        rows = send_ref.shape[0]
-        number = lax.broadcasted_iota(jnp.int32, (rows, tokens.shape[0]), 0) + block * rows
-        chosen = sum((b * rows + p == number).astype(F32) for b, p in places)
-        send_ref[...] = mm(chosen.astype(BF16), normed, 1, 0).astype(BF16)
+    number = lax.broadcasted_iota(jnp.int32, chosen_ref.shape, 0)
+    chosen_ref[...] = sum((b * rows + p == number).astype(F32) for b, p in places).astype(BF16)
+    width = 512
+
+    def columns(c, _):
+        cols = pl.ds(pl.multiple_of(c * width, width), width)
+        sent = mm(chosen_ref[...], normed_ref[:, cols], 1, 0).astype(BF16)
+        near_ref[:, cols] = sent[:rows]
+        others_ref[:rows, cols] = sent[rows : 2 * rows]
+        late_ref[:, cols] = sent[2 * rows : 3 * rows]
+        others_ref[rows:, cols] = sent[3 * rows :]
+        return 0
+
+    lax.fori_loop(0, near_ref.shape[1] // width, columns, 0)
 
 
 def dispatch(core, tokens, gain, routes, experts):
     rows = experts // 2 * TILE
+    count, features = tokens.shape
     return pl.pallas_call(
         functools.partial(dispatch_kernel, experts),
         in_specs=[SMEM, VMEM, VMEM, VMEM],
-        out_specs=[VMEM] * 4,
-        out_shape=[jax.ShapeDtypeStruct((rows, tokens.shape[1]), BF16)] * 4,
+        out_specs=[VMEM] * 3,
+        out_shape=[jax.ShapeDtypeStruct((n * rows, features), BF16) for n in (1, 2, 1)],
+        scratch_shapes=[pltpu.VMEM((count, features), BF16), pltpu.VMEM((4 * rows, count), BF16)],
         cost_estimate=pl.CostEstimate(
             flops=8 * tokens.size * rows, bytes_accessed=10 * tokens.size, transcendentals=0
         ),
@@ -350,7 +364,7 @@
     weights = weight_ref[...]
     tokens = weights.shape[1]
     places = slots_of(route_ref[...], core_ref[0], experts)
-    total = base_ref[...] if first else 0.0
+    parts = []
     for block, ref in enumerate(back_refs, first):
         rows = ref.shape[0]
         number = lax.broadcasted_iota(jnp.int32, (rows, tokens), 0) + block * rows
@@ -359,9 +373,18 @@
             for k, (b, p) in enumerate(places)
         )
         high = mixed.astype(BF16)
-        low = (mixed - high.astype(F32)).astype(BF16)
-        total = total + (mm(high, ref[...], 0, 0) + mm(low, ref[...], 0, 0))
-    out_ref[...] = total.astype(out_ref.dtype)
+        parts += [(high, ref), ((mixed - high.astype(F32)).astype(BF16), ref)]
+    width = 512
+
+    def columns(c, _):
+        cols = pl.ds(pl.multiple_of(c * width, width), width)
+        total = base_ref[:, cols] if first else 0.0
+        for mixed, ref in parts:
+            total = total + mm(mixed, ref[:, cols], 0, 0)
+        out_ref[:, cols] = total.astype(out_ref.dtype)
+        return 0
+
+    lax.fori_loop(0, out_ref.shape[1] // width, columns, 0)
 
 
 def combine(core, weights, routes, experts, returned, first=0, base=()):
@@ -401,7 +424,14 @@
     gate_pre = mm(rows, gate_ref[...], 1, 0)
     up_pre = mm(rows, up_ref[...], 1, 0)
     hidden = clamped_unit(gate_pre, up_pre).astype(BF16)
-    total_ref[...] += mm(hidden, down_ref[...], 1, 0)
+    part = 512
+
+    def columns(c, _):
+        cols = pl.ds(pl.multiple_of(c * part, part), part)
+        total_ref[:, cols] += mm(hidden, down_ref[:, cols], 1, 0)
+        return 0
+
+    lax.fori_loop(0, total_ref.shape[1] // part, columns, 0)
 
     @pl.when(step == pl.num_programs(0) - 1)
     def _():
@@ -511,17 +541,12 @@
     me = lax.axis_index("tp").astype(jnp.int32).reshape(1)
     place = jnp.stack([core[0], lax.axis_index("tp").astype(jnp.int32)])
 
-    half = mixer_output_weight.shape[0] // 2
-    weight_part = lax.dynamic_slice_in_dim(mixer_output_weight, core[0] * half, half, 0)
-    weight_mine = lax.all_gather(weight_part, "tp", axis=0, tiled=False)
-    weight_other = turned(weight_mine, "ep_1", 1)
+    weights_all = gathered_pieces(mixer_output_weight)
 
     routes_t, weights_t = jnp.transpose(routes), jnp.transpose(chosen_expert_weight)
-    near, far, late_near, late_far = dispatch(
-        core, after(second_batch_tokens, weight_part), expert_norm_gain, routes_t, n_ep
-    )
-    far = turned(far, "ep_1", 1)
-    late = late_near + turned(late_far, "ep_1", 1)
+    near, others, late_near = dispatch(core, second_batch_tokens, expert_norm_gain, routes_t, n_ep)
+    others = turned(others, "ep_1", 1)
+    far, late = others[: near.shape[0]], late_near + others[near.shape[0] :]
 
     state = mixer_states(
         forget_gate_logits, value, forget_lower_margin, position_log_decay
@@ -538,7 +563,7 @@
         arrived = sent_over_chips(rows, chips)
         pieces = gathered_pieces(arrived)
         if not c:
-            pieces = after(pieces, weight_mine)
+            pieces = after(pieces, weights_all)
         parts = expert_parts(
             me,
             pieces,
@@ -579,7 +604,7 @@
         turned(heads[owners - 1], "tp", -1),
         turned(heads[2], "tp", 2),
     )
-    first_mixer_output = project(place, heads, weight_mine, weight_other)
+    first_mixer_output = project(heads, weights_all)
 
     back_near, back_far, back_late = returned
     base = combine(core, weights_t, routes_t, n_ep, (back_near, turned(back_far, "ep_1", 1)))

time: 424 us -> 452 us (1.066)
  waiting for transfers between devices: 145 us -> 165 us
  blocking collectives: 64 us -> 71.8 us
  Pallas kernels: 69.2 us -> 74.9 us
    ppermute x26 -> x28, waiting for transfers between devices: 65.5 us -> 86.7 us  [turned(): return lax.ppermute(x, axis, [(i, (i + by) % size) for i in range(size)])]
    all_to_all x2, blocking collectives: 64 us -> 71.8 us  [sent_over_chips(): lax.all_to_all(blocks, 'ep_0', split_axis=0, concat_axis=0, tiled=True)]
    ppermute x26 -> x28, starting transfers between devices: 43.2 us -> 42.1 us  [turned(): return lax.ppermute(x, axis, [(i, (i + by) % size) for i in range(size)])]
  transfers between devices with their start and end apart: 34 -> 35, of which waited for: 18 -> 19; matrix products, arithmetic and copies ran while one was open for 2% -> 2% of each run, Pallas kernels for 15% -> 13%
where the time goes in v1:
time: 452 us; the launch traced here: 451 us
  waiting for transfers between devices  165 us (37%)
  starting transfers between devices  107 us (24%)
  Pallas kernels  74.9 us (17%)
  blocking collectives  71.8 us (16%)
  between operations  15.8 us (3%)
  local copies, waits for them, and re-layouts  11.7 us (3%)
    ppermute x28, waiting for transfers between devices, turned(): return lax.ppermute(x, axis, [(i, (i + by) % size) for i in range(size)])  86.7 us
    all_to_all x2, blocking collectives, sent_over_chips(): lax.all_to_all(blocks, 'ep_0', split_axis=0, concat_axis=0, tiled=True)  71.8 us
    all_to_all x4, starting transfers between devices, sent_over_chips(): lax.all_to_all(blocks, 'ep_0', split_axis=0, concat_axis=0, tiled=True)  65 us
    all_gather x1, waiting for transfers between devices, body(): gathered = lax.all_gather(chip_state, 'ep_0', axis=0, tiled=False)  57.1 us
    ppermute x28, starting transfers between devices, turned(): return lax.ppermute(x, axis, [(i, (i + by) % size) for i in range(size)])  42.1 us
    pallas_call x3, Pallas kernels, expert_parts(): pl.pallas_call(functools.partial(expert_kernel, len(pieces)), grid=(hidde...  29.2 us
    all_to_all x4, waiting for transfers between devices, sent_over_chips(): lax.all_to_all(blocks, 'ep_0', split_axis=0, concat_axis=0, tiled=True)  21.5 us
    pallas_call x1, Pallas kernels, mixer_heads(): pl.pallas_call(heads_kernel, in_specs=[SMEM] + [VMEM] * 9, out_specs=VMEM...  13.2 us
  transfers between devices with their start and end apart: 35, of which 19 were waited for; matrix products, arithmetic and copies ran while one was open for 2% of the time, Pallas kernels for 13%

profile of v1, /device:TPU:33, one launch (start us, length us, event | category | flops | bytes accessed | tf_op | source)
XLA Modules:
  0.0 451.0 jit_solution(11979836737996655353)
XLA Ops:
  8.0 3.8 dispatch_rows.1
  11.8 24.5 %all-to-all-start = ((bf16[16,8,2048]{2,1,0:T(8,128)(2,1)}), bf16[16,8,2048]{2,1,0:T(8,128)(2,1)S(1)}, u32[]{:S(2)}, u32[]{:S(2)}) async-start(bf16[16,8,2048]{2,1,0:T(8,128)(2,1)} %bitcast.50), calls=%async_computation | async-start | bytes 1048576 | tf_op jit(solution)/shard_map/all_to_all | solution.py:513
  36.4 1.0 collective-permute-start.17
  37.4 2.5 collective-permute-done.17
  39.9 1.9 fusion
  41.8 17.3 %all-to-all-done = bf16[16,8,2048]{2,1,0:T(8,128)(2,1)S(1)} async-done(((bf16[16,8,2048]{2,1,0:T(8,128)(2,1)}), bf16[16,8,2048]{2,1,0:T(8,128)(2,1)S(1)}, u32[]{:S(2)}, u32[]{:S(2)}) %all-to-all-start) | async-done | bytes 524320 | tf_op jit(solution)/shard_map/all_to_all | solution.py:513
  59.1 35.3 %all_to_all.30 = bf16[16,8,2048]{2,1,0:T(8,128)(2,1)S(1)} all-to-all(bf16[16,8,2048]{2,1,0:T(8,128)(2,1)S(1)} %bitcast.35), channel_id=1, replica_groups=mesh['grp'=2,'ep_0'=16,'ep_1'=2,'tp'=4] {'ep_0'}, dimensions={0} | all-to-all | bytes 1048576 | tf_op jit(solution)/shard_map/all_to_all | solution.py:513
  94.4 2.9 collective-permute-start.19
  97.3 6.1 %collective-permute-done.19.refs_2_ = bf16[128,2048]{1,0:T(8,128)(2,1)S(1)} collective-permute-done((bf16[128,2048]{1,0:T(8,128)(2,1)S(1)}, bf16[128,2048]{1,0:T(8,128)(2,1)S(1)}, u32[]{:S(2)}, u32[]{:S(2)}) %collective-permute-start.19) | collective-permute-done | bytes 524320 | tf_op jit(solution)/shard_map/ppermute | solution.py:485
  103.4 3.2 collective-permute-start.21
  106.8 6.0 %collective-permute-done.21.refs_4_ = bf16[64,2048]{1,0:T(8,128)(2,1)S(1)} collective-permute-done((bf16[64,2048]{1,0:T(8,128)(2,1)S(1)}, bf16[64,2048]{1,0:T(8,128)(2,1)S(1)}, u32[]{:S(2)}, u32[]{:S(2)}) %collective-permute-start.21) | collective-permute-done | bytes 262176 | tf_op jit(solution)/shard_map/ppermute | solution.py:485
  112.8 3.5 collective-permute-done.20.refs_3_
  116.3 0.7 copy-done.26
  117.0 9.7 %expert_parts.4 = bf16[4,128,2048]{2,1,0:T(8,128)(2,1)} custom-call(s32[1]{0:T(128)} %bitcast.1.me_ref, bf16[2048,512]{1,0:T(8,128)(2,1)} %bitcast.56, bf16[2048,512]{1,0:T(8,128)(2,1)} %bitcast.59, bf16[512,2048]{1,0:T(8,128)(2,1)} %bitcast.62, bf16[128,2048]{1,0:T(8,128)(2,1)} %bitcast.49, bf16[128,2048]{1,0:T(8,128)(2,1)} %copy-done.21, ...), custom_call_target="tpu_custom_call" | custom-call | flops 3221225472 | bytes 10485760 | tf_op jit(solution)/shard_map/expert_parts/pallas_call | solution.py:461
  126.8 1.2 copy-done.3
  128.0 1.5 collective-permute-start.5
  129.4 15.5 %all-to-all-start.2 = ((bf16[16,8,2048]{2,1,0:T(8,128)(2,1)}), bf16[16,8,2048]{2,1,0:T(8,128)(2,1)}, u32[]{:S(2)}, u32[]{:S(2)}) async-start(bf16[16,8,2048]{2,1,0:T(8,128)(2,1)} %bitcast.19), calls=%async_computation.2 | async-start | bytes 1048576 | tf_op jit(solution)/shard_map/all_to_all | solution.py:513
  145.0 1.6 collective-permute-start.10
  146.6 3.0 collective-permute-start.8
  149.8 20.4 %collective-permute-done.10.refs_2_ = bf16[128,2048]{1,0:T(8,128)(2,1)S(1)} collective-permute-done((bf16[128,2048]{1,0:T(8,128)(2,1)}, bf16[128,2048]{1,0:T(8,128)(2,1)S(1)}, u32[]{:S(2)}, u32[]{:S(2)}) %collective-permute-start.10) | collective-permute-done | bytes 524320 | tf_op jit(solution)/shard_map/ppermute | solution.py:485
  170.2 3.1 collective-permute-start.12
  173.5 13.9 %collective-permute-done.8.refs_4_ = bf16[128,2048]{1,0:T(8,128)(2,1)S(1)} collective-permute-done((bf16[128,2048]{1,0:T(8,128)(2,1)S(1)}, bf16[128,2048]{1,0:T(8,128)(2,1)S(1)}, u32[]{:S(2)}, u32[]{:S(2)}) %collective-permute-start.8) | collective-permute-done | bytes 524320 | tf_op jit(solution)/shard_map/ppermute | solution.py:485
  187.4 2.0 collective-permute-done.7.refs_3_
  189.3 3.7 collective-permute-done.12.refs_4_
  193.0 1.9 collective-permute-done.11.refs_3_
  195.0 0.7 copy-done.24
  195.6 9.7 %expert_parts.3 = (bf16[128,2048]{1,0:T(8,128)(2,1)}, bf16[128,2048]{1,0:T(8,128)(2,1)}, bf16[128,2048]{1,0:T(8,128)(2,1)}, bf16[64,2048]{1,0:T(8,128)(2,1)}, bf16[64,2048]{1,0:T(8,128)(2,1)}) custom-call(s32[1]{0:T(128)} %bitcast.1.me_ref, bf16[2048,512]{1,0:T(8,128)(2,1)} %bitcast.57, bf16[2048,512]{1,0:T(8,128)(2,1)} %bitcast.60, ...), custom_call_target="tpu_custom_call" | custom-call | flops 3221225472 | bytes 10485760 | tf_op jit(solution)/shard_map/expert_parts/pallas_call | solution.py:461
  205.4 1.0 collective-permute-start.15
  206.4 1.0 slice.62
  207.4 1.0 slice.65
  208.4 0.7 collective-permute-start.13
  209.0 1.9 collective-permute-done.15
  210.9 1.0 add_convert_fusion.1
  212.0 2.2 collective-permute-start.24
  214.3 2.8 collective-permute-start.16
  217.1 4.9 %collective-permute-done.24.refs_2_ = bf16[128,2048]{1,0:T(8,128)(2,1)S(1)} collective-permute-done((bf16[128,2048]{1,0:T(8,128)(2,1)}, bf16[128,2048]{1,0:T(8,128)(2,1)S(1)}, u32[]{:S(2)}, u32[]{:S(2)}) %collective-permute-start.24) | collective-permute-done | bytes 524320 | tf_op jit(solution)/shard_map/ppermute | solution.py:485
  222.1 1.7 collective-permute-start.26
  223.8 4.0 collective-permute-done.23.refs_1_
  228.4 9.8 %collective-permute-done.26.refs_4_ = bf16[64,2048]{1,0:T(8,128)(2,1)S(1)} collective-permute-done((bf16[64,2048]{1,0:T(8,128)(2,1)S(1)}, bf16[64,2048]{1,0:T(8,128)(2,1)S(1)}, u32[]{:S(2)}, u32[]{:S(2)}) %collective-permute-start.26) | collective-permute-done | bytes 262176 | tf_op jit(solution)/shard_map/ppermute | solution.py:485
  238.2 0.7 copy-done.23
  238.9 9.7 %expert_parts.5 = bf16[4,128,2048]{2,1,0:T(8,128)(2,1)} custom-call(s32[1]{0:T(128)} %bitcast.1.me_ref, bf16[2048,512]{1,0:T(8,128)(2,1)} %bitcast.58, bf16[2048,512]{1,0:T(8,128)(2,1)} %bitcast.61, bf16[512,2048]{1,0:T(8,128)(2,1)} %bitcast.64, bf16[128,2048]{1,0:T(8,128)(2,1)} %bitcast.20.refs_0_, bf16[128,2048]{1,0:T(8,128)(2,1)} %copy-done.19, ...), custom_call_target="tpu_custom_call" | custom-call | flops 3221225472 | bytes 10485760 | tf_op jit(solution)/shard_map/expert_parts/pallas_call | solution.py:461
  248.7 1.0 copy-done.8
  249.9 36.5 %all_to_all.31 = bf16[16,8,2048]{2,1,0:T(8,128)(2,1)} all-to-all(bf16[16,8,2048]{2,1,0:T(8,128)(2,1)S(1)} %bitcast.39), channel_id=1, replica_groups=mesh['grp'=2,'ep_0'=16,'ep_1'=2,'tp'=4] {'ep_0'}, dimensions={0} | all-to-all | bytes 1048576 | tf_op jit(solution)/shard_map/all_to_all | solution.py:513
  286.4 13.0 %all-to-all-start.4 = ((bf16[16,8,2048]{2,1,0:T(8,128)(2,1)}), bf16[16,8,2048]{2,1,0:T(8,128)(2,1)S(1)}, u32[]{:S(2)}, u32[]{:S(2)}) async-start(bf16[16,8,2048]{2,1,0:T(8,128)(2,1)} %bitcast.41), calls=%async_computation.5 | async-start | bytes 1048576 | tf_op jit(solution)/shard_map/all_to_all | solution.py:513
  299.5 10.3 %mixer_states.1.own_ref = bf16[2,2,144,128]{3,2,1,0:T(8,128)(2,1)} custom-call(bf16[1024,256]{1,0:T(8,128)(2,1)} %logits_ref.3, bf16[1024,256]{1,0:T(8,128)(2,1)} %value_ref.3, f32[2,256]{1,0:T(2,128)} %margin_ref.3, f32[2,1024]{1,0:T(2,128)} %decay_ref.3), custom_call_target="tpu_custom_call" | custom-call | flops 805306368 | bytes 1310720 | tf_op jit(solution)/shard_map/mixer_states/pallas_call | solution.py:107
  309.8 4.0 collective-permute-start
  313.8 1.2 collective-permute-done.partner_ref
  315.7 1.7 mixer_merge.1
  317.4 4.2 all-to-all-done.4
  321.6 11.9 %all-to-all-start.5 = ((bf16[16,8,2048]{2,1,0:T(8,128)(2,1)}), bf16[16,8,2048]{2,1,0:T(8,128)(2,1)S(1)}, u32[]{:S(2)}, u32[]{:S(2)}) async-start(bf16[16,8,2048]{2,1,0:T(8,128)(2,1)} %bitcast.46), calls=%async_computation.7 | async-start | bytes 1048576 | tf_op jit(solution)/shard_map/all_to_all | solution.py:513
  333.5 57.1 %all-gather.3.cloned.1.call-done = bf16[32,144,128]{2,1,0:T(8,128)(2,1)} async-done(((bf16[2,144,128]{2,1,0:T(8,128)(2,1)}), bf16[32,144,128]{2,1,0:T(8,128)(2,1)}) %all-gather.3.cloned.1.call-update) | async-done | bytes 1179664 | tf_op jit(solution)/shard_map/all_gather | solution.py:556
  390.6 2.6 mixer_entering.1.mine_ref
  393.2 6.8 %collective-permute-start.1 = (bf16[2,128,128]{2,1,0:T(8,128)(2,1)}, bf16[2,128,128]{2,1,0:T(8,128)(2,1)S(1)}, u32[]{:S(2)}, u32[]{:S(2)}) collective-permute-start(bf16[2,128,128]{2,1,0:T(8,128)(2,1)} %mixer_entering.1.mine_ref), channel_id=1, source_target_pairs={{0,4},{4,0},{1,5},{5,1},{2,6},{6,2},{3,7},{7,3},{8,12},{12,8},{9,1... | collective-permute-start | bytes 196616 | tf_op jit(solution)/shard_map/ppermute | solution.py:485
  401.8 13.2 %mixer_heads.1 = bf16[4,2,256,128]{3,2,1,0:T(8,128)(2,1)} custom-call(s32[2]{0:T(128)} %pad_add_fusion.place_ref, bf16[1024,256]{1,0:T(8,128)(2,1)} %query_ref.1, bf16[1024,256]{1,0:T(8,128)(2,1)} %logits_ref.3, bf16[1024,256]{1,0:T(8,128)(2,1)} %value_ref.3, f32[2,256]{1,0:T(2,128)} %margin_ref.3, f32[2,1024]{1,0:T(2,128)} %decay_ref.3, f32[1,128]{1,0:T(1,128)} %bitcast.66, ...), custom_call_target="tpu_custom_call" | custom-call | flops 1610612736 | bytes 4194304 | tf_op jit(solution)/shard_map/mixer_heads/pallas_call | solution.py:255
  414.9 1.8 slice_bitcast_fusion
  416.7 3.8 collective-permute-start.4
  420.6 1.4 collective-permute-start.2
  422.0 2.1 collective-permute-done.4.far_ref
  424.1 2.8 collective-permute-done.3.right_ref
  427.6 6.8 %mixer_project.1 = bf16[256,2048]{1,0:T(8,128)(2,1)} custom-call(bf16[2,256,128]{2,1,0:T(8,128)(2,1)} %get-tuple-element.43.own_ref, bf16[2,256,128]{2,1,0:T(8,128)(2,1)} %copy-done.15, bf16[2,256,128]{2,1,0:T(8,128)(2,1)} %copy-done.14, bf16[2,256,128]{2,1,0:T(8,128)(2,1)} %copy-done.13, bf16[256,2048]{1,0:T(8,128)(2,1)} %refs_0_.1, ...), custom_call_target="tpu_custom_call" | custom-call | flops 1073741824 | bytes 4194304 | tf_op jit(solution)/shard_map/mixer_project/pallas_call | solution.py:289
  434.4 0.8 copy-done.9
  435.2 3.7 combine_rows.2.refs_0_
  438.9 0.8 copy-done.4
  439.7 3.8 combine_rows.3
  (96 shorter events, 5.1 us)
Async XLA Ops:
  11.8 47.3 %all-to-all-start = ((bf16[16,8,2048]{2,1,0:T(8,128)(2,1)}), bf16[16,8,2048]{2,1,0:T(8,128)(2,1)S(1)}, u32[]{:S(2)}, u32[]{:S(2)}) async-start(bf16[16,8,2048]{2,1,0:T(8,128)(2,1)} %bitcast.50), calls=%async_computation | async-start | bytes 1048576 | tf_op jit(solution)/shard_map/all_to_all | solution.py:513
  36.3 250.1 %reduce-scatter.3.cloned.1.call-start = ((), (), s32[]{:S(2)}) async-start(), calls=%async_computation.8 | async-start | bytes 2621440 | tf_op jit(solution)/shard_map/reduce_scatter | solution.py:577
  36.4 3.5 collective-permute-start.17
  59.1 67.7 %copy-start.6 = (bf16[16,8,2048]{2,1,0:T(8,128)(2,1)}, bf16[16,8,2048]{2,1,0:T(8,128)(2,1)S(1)}, u32[]{:S(2)}) copy-start(bf16[16,8,2048]{2,1,0:T(8,128)(2,1)S(1)} %all-to-all-done) | copy-start | bytes 1572868
  94.4 21.9 %copy-start.7 = (bf16[16,8,2048]{2,1,0:T(8,128)(2,1)}, bf16[16,8,2048]{2,1,0:T(8,128)(2,1)S(1)}, u32[]{:S(2)}) copy-start(bf16[16,8,2048]{2,1,0:T(8,128)(2,1)S(1)} %all_to_all.30) | copy-start | bytes 1572868
  94.4 9.0 %collective-permute-start.19 = (bf16[128,2048]{1,0:T(8,128)(2,1)S(1)}, bf16[128,2048]{1,0:T(8,128)(2,1)S(1)}, u32[]{:S(2)}, u32[]{:S(2)}) collective-permute-start(bf16[128,2048]{1,0:T(8,128)(2,1)S(1)} %bitcast.47), channel_id=1, source_target_pairs={{0,3},{1,0},{2,1},{3,2},{4,7},{5,4},{6,5},{7,6},{8,11},{9,8},{10,9... | collective-permute-start | bytes 1572872 | tf_op jit(solution)/shard_map/ppermute | solution.py:485
  97.3 9.4 %collective-permute-start.18 = (bf16[128,2048]{1,0:T(8,128)(2,1)S(1)}, bf16[128,2048]{1,0:T(8,128)(2,1)S(1)}, u32[]{:S(2)}, u32[]{:S(2)}) collective-permute-start(bf16[128,2048]{1,0:T(8,128)(2,1)S(1)} %bitcast.48), channel_id=1, source_target_pairs={{0,1},{1,2},{2,3},{3,0},{4,5},{5,6},{6,7},{7,4},{8,9},{9,10},{10,1... | collective-permute-start | bytes 1572872 | tf_op jit(solution)/shard_map/ppermute | solution.py:485
  103.4 12.9 %copy-start.20 = (bf16[128,2048]{1,0:T(8,128)(2,1)}, bf16[128,2048]{1,0:T(8,128)(2,1)S(1)}, u32[]{:S(2)}) copy-start(bf16[128,2048]{1,0:T(8,128)(2,1)S(1)} %collective-permute-done.19.refs_2_) | copy-start | bytes 1572868
  103.4 9.4 %collective-permute-start.21 = (bf16[64,2048]{1,0:T(8,128)(2,1)S(1)}, bf16[64,2048]{1,0:T(8,128)(2,1)S(1)}, u32[]{:S(2)}, u32[]{:S(2)}) collective-permute-start(bf16[64,2048]{1,0:T(8,128)(2,1)S(1)} %slice.83), channel_id=1, source_target_pairs={{0,3},{1,0},{2,1},{3,2},{4,7},{5,4},{6,5},{7,6},{8,11},{9,8},{10,9... | collective-permute-start | bytes 786440 | tf_op jit(solution)/shard_map/ppermute | solution.py:485
  106.6 9.7 %copy-start.21 = (bf16[128,2048]{1,0:T(8,128)(2,1)}, bf16[128,2048]{1,0:T(8,128)(2,1)S(1)}, u32[]{:S(2)}) copy-start(bf16[128,2048]{1,0:T(8,128)(2,1)S(1)} %collective-permute-done.18.refs_1_) | copy-start | bytes 1572868
  106.7 9.6 %collective-permute-start.20 = (bf16[64,2048]{1,0:T(8,128)(2,1)S(1)}, bf16[64,2048]{1,0:T(8,128)(2,1)S(1)}, u32[]{:S(2)}, u32[]{:S(2)}) collective-permute-start(bf16[64,2048]{1,0:T(8,128)(2,1)S(1)} %slice.82), channel_id=1, source_target_pairs={{0,1},{1,2},{2,3},{3,0},{4,5},{5,6},{6,7},{7,4},{8,9},{9,10},{10,1... | collective-permute-start | bytes 786440 | tf_op jit(solution)/shard_map/ppermute | solution.py:485
  112.8 3.6 copy-start.25
  116.3 0.7 copy-start.26
  126.7 1.2 copy-start.3
  128.0 18.6 %collective-permute-start.6 = (bf16[256,2048]{1,0:T(8,128)(2,1)S(1)}, bf16[256,2048]{1,0:T(8,128)(2,1)S(1)}, u32[]{:S(2)}, u32[]{:S(2)}) collective-permute-start(bf16[256,2048]{1,0:T(8,128)(2,1)S(1)} %copy-done.3), channel_id=1, source_target_pairs={{0,3},{1,0},{2,1},{3,2},{4,7},{5,4},{6,5},{7,6},{8,11},{9,8},{10,9... | collective-permute-start | bytes 3145736 | tf_op jit(solution)/shard_map/ppermute | solution.py:485
  128.0 21.6 %collective-permute-start.5 = (bf16[256,2048]{1,0:T(8,128)(2,1)S(1)}, bf16[256,2048]{1,0:T(8,128)(2,1)S(1)}, u32[]{:S(2)}, u32[]{:S(2)}) collective-permute-start(bf16[256,2048]{1,0:T(8,128)(2,1)S(1)} %copy-done.3), channel_id=1, source_target_pairs={{0,1},{1,2},{2,3},{3,0},{4,5},{5,6},{6,7},{7,4},{8,9},{9,10},{10,1... | collective-permute-start | bytes 3145736 | tf_op jit(solution)/shard_map/ppermute | solution.py:485
  129.4 82.5 %all-to-all-start.2 = ((bf16[16,8,2048]{2,1,0:T(8,128)(2,1)}), bf16[16,8,2048]{2,1,0:T(8,128)(2,1)}, u32[]{:S(2)}, u32[]{:S(2)}) async-start(bf16[16,8,2048]{2,1,0:T(8,128)(2,1)} %bitcast.19), calls=%async_computation.2 | async-start | bytes 1048576 | tf_op jit(solution)/shard_map/all_to_all | solution.py:513
  144.9 172.5 %reduce-scatter.5.cloned.1.call-start = ((), (), s32[]{:S(2)}) async-start(), calls=%async_computation.9 | async-start | bytes 2621440 | tf_op jit(solution)/shard_map/reduce_scatter | solution.py:577
  145.0 25.1 %collective-permute-start.10 = (bf16[128,2048]{1,0:T(8,128)(2,1)}, bf16[128,2048]{1,0:T(8,128)(2,1)S(1)}, u32[]{:S(2)}, u32[]{:S(2)}) collective-permute-start(bf16[128,2048]{1,0:T(8,128)(2,1)} %bitcast.42), channel_id=1, source_target_pairs={{0,3},{1,0},{2,1},{3,2},{4,7},{5,4},{6,5},{7,6},{8,11},{9,8},{10,9... | collective-permute-start | bytes 1572872 | tf_op jit(solution)/shard_map/ppermute | solution.py:485
  146.6 26.7 %collective-permute-start.9 = (bf16[128,2048]{1,0:T(8,128)(2,1)}, bf16[128,2048]{1,0:T(8,128)(2,1)S(1)}, u32[]{:S(2)}, u32[]{:S(2)}) collective-permute-start(bf16[128,2048]{1,0:T(8,128)(2,1)} %bitcast.43), channel_id=1, source_target_pairs={{0,1},{1,2},{2,3},{3,0},{4,5},{5,6},{6,7},{7,4},{8,9},{9,10},{10,1... | collective-permute-start | bytes 1572872 | tf_op jit(solution)/shard_map/ppermute | solution.py:485
  146.6 58.8 %copy-start = (bf16[256,2048]{1,0:T(8,128)(2,1)}, bf16[256,2048]{1,0:T(8,128)(2,1)S(1)}, u32[]{:S(2)}) copy-start(bf16[256,2048]{1,0:T(8,128)(2,1)S(1)} %collective-permute-done.6.refs_2_) | copy-start | bytes 3145732
  146.6 40.7 %collective-permute-start.8 = (bf16[128,2048]{1,0:T(8,128)(2,1)S(1)}, bf16[128,2048]{1,0:T(8,128)(2,1)S(1)}, u32[]{:S(2)}, u32[]{:S(2)}) collective-permute-start(bf16[128,2048]{1,0:T(8,128)(2,1)S(1)} %slice.77), channel_id=1, source_target_pairs={{0,3},{1,0},{2,1},{3,2},{4,7},{5,4},{6,5},{7,6},{8,11},{9,8},{10,9... | collective-permute-start | bytes 1572872 | tf_op jit(solution)/shard_map/ppermute | solution.py:485
  149.6 55.8 %copy-start.1 = (bf16[256,2048]{1,0:T(8,128)(2,1)}, bf16[256,2048]{1,0:T(8,128)(2,1)S(1)}, u32[]{:S(2)}) copy-start(bf16[256,2048]{1,0:T(8,128)(2,1)S(1)} %collective-permute-done.5.refs_1_) | copy-start | bytes 3145732
  149.7 39.7 %collective-permute-start.7 = (bf16[128,2048]{1,0:T(8,128)(2,1)S(1)}, bf16[128,2048]{1,0:T(8,128)(2,1)S(1)}, u32[]{:S(2)}, u32[]{:S(2)}) collective-permute-start(bf16[128,2048]{1,0:T(8,128)(2,1)S(1)} %slice.76), channel_id=1, source_target_pairs={{0,1},{1,2},{2,3},{3,0},{4,5},{5,6},{6,7},{7,4},{8,9},{9,10},{10,1... | collective-permute-start | bytes 1572872 | tf_op jit(solution)/shard_map/ppermute | solution.py:485
  170.2 22.8 %copy-start.16 = (bf16[128,2048]{1,0:T(8,128)(2,1)}, bf16[128,2048]{1,0:T(8,128)(2,1)S(1)}, u32[]{:S(2)}) copy-start(bf16[128,2048]{1,0:T(8,128)(2,1)S(1)} %collective-permute-done.10.refs_2_) | copy-start | bytes 1572868
  170.2 22.8 %collective-permute-start.12 = (bf16[64,2048]{1,0:T(8,128)(2,1)S(1)}, bf16[64,2048]{1,0:T(8,128)(2,1)S(1)}, u32[]{:S(2)}, u32[]{:S(2)}) collective-permute-start(bf16[64,2048]{1,0:T(8,128)(2,1)S(1)} %slice.79), channel_id=1, source_target_pairs={{0,3},{1,0},{2,1},{3,2},{4,7},{5,4},{6,5},{7,6},{8,11},{9,8},{10,9... | collective-permute-start | bytes 786440 | tf_op jit(solution)/shard_map/ppermute | solution.py:485
  173.3 19.7 %copy-start.17 = (bf16[128,2048]{1,0:T(8,128)(2,1)}, bf16[128,2048]{1,0:T(8,128)(2,1)S(1)}, u32[]{:S(2)}) copy-start(bf16[128,2048]{1,0:T(8,128)(2,1)S(1)} %collective-permute-done.9.refs_1_) | copy-start | bytes 1572868
  173.3 21.6 %collective-permute-start.11 = (bf16[64,2048]{1,0:T(8,128)(2,1)S(1)}, bf16[64,2048]{1,0:T(8,128)(2,1)S(1)}, u32[]{:S(2)}, u32[]{:S(2)}) collective-permute-start(bf16[64,2048]{1,0:T(8,128)(2,1)S(1)} %slice.78), channel_id=1, source_target_pairs={{0,1},{1,2},{2,3},{3,0},{4,5},{5,6},{6,7},{7,4},{8,9},{9,10},{10,1... | collective-permute-start | bytes 786440 | tf_op jit(solution)/shard_map/ppermute | solution.py:485
  187.4 2.0 copy-start.10
  189.3 3.7 copy-start.11
  193.0 2.0 copy-start.22
  194.9 0.7 copy-start.24
  205.4 11.7 %copy-start.5 = (bf16[128,2048]{1,0:T(8,128)(2,1)S(1)}, bf16[128,2048]{1,0:T(8,128)(2,1)}, u32[]{:S(2)}) copy-start(bf16[128,2048]{1,0:T(8,128)(2,1)} %get-tuple-element.27) | copy-start | bytes 1572868
  205.4 5.5 %collective-permute-start.15 = (bf16[64,2048]{1,0:T(8,128)(2,1)}, bf16[64,2048]{1,0:T(8,128)(2,1)S(1)}, u32[]{:S(2)}, u32[]{:S(2)}) collective-permute-start(bf16[64,2048]{1,0:T(8,128)(2,1)} %get-tuple-element.30), channel_id=1, source_target_pairs={{0,3},{1,0},{2,1},{3,2},{4,7},{5,4},{6,5},{7,6},{8,11},{9,8},{10,9... | collective-permute-start | bytes 786440 | tf_op jit(solution)/shard_map/ppermute | solution.py:485
  208.4 8.7 %collective-permute-start.13 = (bf16[64,2048]{1,0:T(8,128)(2,1)}, bf16[64,2048]{1,0:T(8,128)(2,1)S(1)}, u32[]{:S(2)}, u32[]{:S(2)}) collective-permute-start(bf16[64,2048]{1,0:T(8,128)(2,1)} %get-tuple-element.28), channel_id=1, source_target_pairs={{0,1},{1,2},{2,3},{3,0},{4,5},{5,6},{6,7},{7,4},{8,9},{9,10},{10,1... | collective-permute-start | bytes 786440 | tf_op jit(solution)/shard_map/ppermute | solution.py:485
  212.0 10.1 %collective-permute-start.24 = (bf16[128,2048]{1,0:T(8,128)(2,1)}, bf16[128,2048]{1,0:T(8,128)(2,1)S(1)}, u32[]{:S(2)}, u32[]{:S(2)}) collective-permute-start(bf16[128,2048]{1,0:T(8,128)(2,1)} %bitcast.20.refs_0_), channel_id=1, source_target_pairs={{0,3},{1,0},{2,1},{3,2},{4,7},{5,4},{6,5},{7,6},{8,11},{9,8},{10,9... | collective-permute-start | bytes 1572872 | tf_op jit(solution)/shard_map/ppermute | solution.py:485
  214.2 13.6 %collective-permute-start.23 = (bf16[128,2048]{1,0:T(8,128)(2,1)}, bf16[128,2048]{1,0:T(8,128)(2,1)S(1)}, u32[]{:S(2)}, u32[]{:S(2)}) collective-permute-start(bf16[128,2048]{1,0:T(8,128)(2,1)} %bitcast.20.refs_0_), channel_id=1, source_target_pairs={{0,1},{1,2},{2,3},{3,0},{4,5},{5,6},{6,7},{7,4},{8,9},{9,10},{10,1... | collective-permute-start | bytes 1572872 | tf_op jit(solution)/shard_map/ppermute | solution.py:485
  214.3 34.4 %collective-permute-start.16 = (bf16[128,2048]{1,0:T(8,128)(2,1)S(1)}, bf16[128,2048]{1,0:T(8,128)(2,1)S(1)}, u32[]{:S(2)}, u32[]{:S(2)}) collective-permute-start(bf16[128,2048]{1,0:T(8,128)(2,1)S(1)} %pad_maximum_fusion.1), channel_id=1, source_target_pairs={{0,3},{1,0},{2,1},{3,2},{4,7},{5,4},{6,5},{7,6},{8,11},{9,8},{10,9... | collective-permute-start | bytes 1572872 | tf_op jit(solution)/shard_map/ppermute | solution.py:485
  222.1 16.1 %copy-start.18 = (bf16[128,2048]{1,0:T(8,128)(2,1)}, bf16[128,2048]{1,0:T(8,128)(2,1)S(1)}, u32[]{:S(2)}) copy-start(bf16[128,2048]{1,0:T(8,128)(2,1)S(1)} %collective-permute-done.24.refs_2_) | copy-start | bytes 1572868
  222.1 16.1 %collective-permute-start.26 = (bf16[64,2048]{1,0:T(8,128)(2,1)S(1)}, bf16[64,2048]{1,0:T(8,128)(2,1)S(1)}, u32[]{:S(2)}, u32[]{:S(2)}) collective-permute-start(bf16[64,2048]{1,0:T(8,128)(2,1)S(1)} %slice.85), channel_id=1, source_target_pairs={{0,3},{1,0},{2,1},{3,2},{4,7},{5,4},{6,5},{7,6},{8,11},{9,8},{10,9... | collective-permute-start | bytes 786440 | tf_op jit(solution)/shard_map/ppermute | solution.py:485
  227.8 10.3 %copy-start.19 = (bf16[128,2048]{1,0:T(8,128)(2,1)}, bf16[128,2048]{1,0:T(8,128)(2,1)S(1)}, u32[]{:S(2)}) copy-start(bf16[128,2048]{1,0:T(8,128)(2,1)S(1)} %collective-permute-done.23.refs_1_) | copy-start | bytes 1572868
  227.9 10.3 %collective-permute-start.25 = (bf16[64,2048]{1,0:T(8,128)(2,1)S(1)}, bf16[64,2048]{1,0:T(8,128)(2,1)}, u32[]{:S(2)}, u32[]{:S(2)}) collective-permute-start(bf16[64,2048]{1,0:T(8,128)(2,1)S(1)} %slice.84), channel_id=1, source_target_pairs={{0,1},{1,2},{2,3},{3,0},{4,5},{5,6},{6,7},{7,4},{8,9},{9,10},{10,1... | collective-permute-start | bytes 786440 | tf_op jit(solution)/shard_map/ppermute | solution.py:485
  228.1 20.6 %collective-permute-start.14 = (bf16[128,2048]{1,0:T(8,128)(2,1)S(1)}, bf16[128,2048]{1,0:T(8,128)(2,1)S(1)}, u32[]{:S(2)}, u32[]{:S(2)}) collective-permute-start(bf16[128,2048]{1,0:T(8,128)(2,1)S(1)} %pad_maximum_fusion), channel_id=1, source_target_pairs={{0,1},{1,2},{2,3},{3,0},{4,5},{5,6},{6,7},{7,4},{8,9},{9,10},{10,1... | collective-permute-start | bytes 1572872 | tf_op jit(solution)/shard_map/ppermute | solution.py:485
  238.2 0.7 copy-start.23
  248.6 1.0 copy-start.8
  286.4 35.2 %all-to-all-start.4 = ((bf16[16,8,2048]{2,1,0:T(8,128)(2,1)}), bf16[16,8,2048]{2,1,0:T(8,128)(2,1)S(1)}, u32[]{:S(2)}, u32[]{:S(2)}) async-start(bf16[16,8,2048]{2,1,0:T(8,128)(2,1)} %bitcast.41), calls=%async_computation.5 | async-start | bytes 1048576 | tf_op jit(solution)/shard_map/all_to_all | solution.py:513
  299.5 91.2 %all-gather.3.cloned.1.call-start = ((), (), s32[]{:S(2)}) async-start(), calls=%async_computation.10 | async-start | bytes 1253376 | tf_op jit(solution)/shard_map/all_gather | solution.py:556
  309.8 5.2 %collective-permute-start = (bf16[2,2,144,128]{3,2,1,0:T(8,128)(2,1)}, bf16[2,2,144,128]{3,2,1,0:T(8,128)(2,1)S(1)}, u32[]{:S(2)}, u32[]{:S(2)}) collective-permute-start(bf16[2,2,144,128]{3,2,1,0:T(8,128)(2,1)} %mixer_states.1.own_ref), channel_id=1, source_target_pairs={{0,4},{4,0},{1,5},{5,1},{2,6},{6,2},{3,7},{7,3},{8,12},{12,8},{9,1... | collective-permute-start | bytes 442376 | tf_op jit(solution)/shard_map/ppermute | solution.py:485
  315.0 0.7 copy-start.12
  321.6 79.0 %all-to-all-start.5 = ((bf16[16,8,2048]{2,1,0:T(8,128)(2,1)}), bf16[16,8,2048]{2,1,0:T(8,128)(2,1)S(1)}, u32[]{:S(2)}, u32[]{:S(2)}) async-start(bf16[16,8,2048]{2,1,0:T(8,128)(2,1)} %bitcast.46), calls=%async_computation.7 | async-start | bytes 1048576 | tf_op jit(solution)/shard_map/all_to_all | solution.py:513
  393.2 7.9 %collective-permute-start.1 = (bf16[2,128,128]{2,1,0:T(8,128)(2,1)}, bf16[2,128,128]{2,1,0:T(8,128)(2,1)S(1)}, u32[]{:S(2)}, u32[]{:S(2)}) collective-permute-start(bf16[2,128,128]{2,1,0:T(8,128)(2,1)} %mixer_entering.1.mine_ref), channel_id=1, source_target_pairs={{0,4},{4,0},{1,5},{5,1},{2,6},{6,2},{3,7},{7,3},{8,12},{12,8},{9,1... | collective-permute-start | bytes 196616 | tf_op jit(solution)/shard_map/ppermute | solution.py:485
  400.6 33.8 %collective-permute-start.22 = (bf16[128,2048]{1,0:T(8,128)(2,1)S(1)}, bf16[128,2048]{1,0:T(8,128)(2,1)S(1)}, u32[]{:S(2)}, u32[]{:S(2)}) collective-permute-start(bf16[128,2048]{1,0:T(8,128)(2,1)S(1)} %bitcast.45), channel_id=1, source_target_pairs={{0,4},{4,0},{1,5},{5,1},{2,6},{6,2},{3,7},{7,3},{8,12},{12,8},{9,1... | collective-permute-start | bytes 1572872 | tf_op jit(solution)/shard_map/ppermute | solution.py:485
  400.6 14.3 %copy-start.2 = (bf16[16,8,2048]{2,1,0:T(8,128)(2,1)}, bf16[16,8,2048]{2,1,0:T(8,128)(2,1)S(1)}, u32[]{:S(2)}) copy-start(bf16[16,8,2048]{2,1,0:T(8,128)(2,1)S(1)} %all-to-all-done.5) | copy-start | bytes 1572868
  400.6 38.3 %collective-permute-start.27 = (bf16[128,2048]{1,0:T(8,128)(2,1)S(1)}, bf16[128,2048]{1,0:T(8,128)(2,1)S(1)}, u32[]{:S(2)}, u32[]{:S(2)}) collective-permute-start(bf16[128,2048]{1,0:T(8,128)(2,1)S(1)} %bitcast.33), channel_id=1, source_target_pairs={{0,4},{4,0},{1,5},{5,1},{2,6},{6,2},{3,7},{7,3},{8,12},{12,8},{9,1... | collective-permute-start | bytes 1572872 | tf_op jit(solution)/shard_map/ppermute | solution.py:485
  401.1 0.6 copy-start.27
  416.7 7.4 %collective-permute-start.4 = (bf16[2,256,128]{2,1,0:T(8,128)(2,1)S(1)}, bf16[2,256,128]{2,1,0:T(8,128)(2,1)S(1)}, u32[]{:S(2)}, u32[]{:S(2)}) collective-permute-start(bf16[2,256,128]{2,1,0:T(8,128)(2,1)S(1)} %get-tuple-element.40), channel_id=1, source_target_pairs={{0,2},{1,3},{2,0},{3,1},{4,6},{5,7},{6,4},{7,5},{8,10},{9,11},{10,... | collective-permute-start | bytes 393224 | tf_op jit(solution)/shard_map/ppermute | solution.py:485
  420.5 6.4 %collective-permute-start.3 = (bf16[2,256,128]{2,1,0:T(8,128)(2,1)S(1)}, bf16[2,256,128]{2,1,0:T(8,128)(2,1)S(1)}, u32[]{:S(2)}, u32[]{:S(2)}) collective-permute-start(bf16[2,256,128]{2,1,0:T(8,128)(2,1)S(1)} %get-tuple-element.41), channel_id=1, source_target_pairs={{0,3},{1,0},{2,1},{3,2},{4,7},{5,4},{6,5},{7,6},{8,11},{9,8},{10,9... | collective-permute-start | bytes 393224 | tf_op jit(solution)/shard_map/ppermute | solution.py:485
  420.6 6.3 %collective-permute-start.2 = (bf16[2,256,128]{2,1,0:T(8,128)(2,1)S(1)}, bf16[2,256,128]{2,1,0:T(8,128)(2,1)S(1)}, u32[]{:S(2)}, u32[]{:S(2)}) collective-permute-start(bf16[2,256,128]{2,1,0:T(8,128)(2,1)S(1)} %get-tuple-element.42), channel_id=1, source_target_pairs={{0,1},{1,2},{2,3},{3,0},{4,5},{5,6},{6,7},{7,4},{8,9},{9,10},{10,1... | collective-permute-start | bytes 393224 | tf_op jit(solution)/shard_map/ppermute | solution.py:485
  424.1 2.8 copy-start.13
  426.9 0.6 copy-start.14
  426.9 0.7 copy-start.15
  434.4 0.8 copy-start.9
  438.9 0.8 copy-start.4
Sparse Core Ops, SparseCore 0:
  126.9 57.1 reduce-scatter.2
  248.8 47.7 reduce-scatter.4
Sparse Core Ops, SparseCore 1:
  317.5 73.1 all-gather.2

commit v2 on v0

--- a/solution.py
+++ b/solution.py
@@ -16,6 +16,7 @@
 GRP_EP = ("grp", "ep_0", "ep_1")
 GRP_EP_TP = ("grp", "ep_0", "ep_1", "tp")
 TILE = 8
+STRIP = 32
 
 NORM_EPS = 1e-06
 CLAMP_LIMIT = 7.0
@@ -265,36 +266,35 @@
     )(place, query, logits, value, margin, decay, gain.reshape(1, HEAD_CHANNELS), mine, other, partner)
 
 
-def project_kernel(place_ref, own_ref, left_ref, right_ref, far_ref, mine_ref, other_ref, out_ref):
-    core, me = place_ref[0], place_ref[1]
-    owners = mine_ref.shape[0]
+def project_kernel(core_ref, own_ref, left_ref, right_ref, far_ref, weight_ref, mine_ref, other_ref, out_ref):
+    core = core_ref[0]
     width = 256
 
     def columns(c, _):
         cols = pl.ds(pl.multiple_of(c * width, width), width)
         total = jnp.zeros((out_ref.shape[0], width), F32)
-        for ref, by in ((own_ref, 0), (left_ref, owners - 1), (right_ref, 1), (far_ref, 2)):
-            source = lax.rem(me + by, owners)
-            total += mm(ref[core], mine_ref[source, :, cols], 1, 0)
-            total += mm(ref[1 - core], other_ref[source, :, cols], 1, 0)
+        for h, (which, ref) in enumerate(((core, mine_ref), (1 - core, other_ref))):
+            total += mm(own_ref[h], weight_ref[columns_of(h), cols], 1, 0)
+            for k, heads_ref in enumerate((left_ref, right_ref, far_ref)):
+                total += mm(heads_ref[which], ref[columns_of(k), cols], 1, 0)
         out_ref[:, cols] = total.astype(BF16)
         return 0
 
     lax.fori_loop(0, out_ref.shape[1] // width, columns, 0)
 
 
-def project(place, heads, mine, other):
-    tokens, features = heads[0].shape[1], mine.shape[2]
+def project(core, heads, weight, mine, other):
+    tokens, features = heads[0].shape[1], weight.shape[1]
     return pl.pallas_call(
         project_kernel,
-        in_specs=[SMEM] + [VMEM] * 6,
+        in_specs=[SMEM] + [VMEM] * 7,
         out_specs=VMEM,
         out_shape=jax.ShapeDtypeStruct((tokens, features), BF16),
         cost_estimate=pl.CostEstimate(
             flops=8 * heads[0].size * features, bytes_accessed=8 * tokens * features, transcendentals=0
         ),
         name="mixer_project",
-    )(place, *heads, mine, other)
+    )(core, *heads, weight, mine, other)
 
 
 def slots_of(routes, core, experts):
@@ -317,16 +317,17 @@
     return result
 
 
-def dispatch_kernel(experts, core_ref, token_ref, gain_ref, route_ref, *send_refs):
+def dispatch_kernel(experts, core_ref, token_ref, gain_ref, route_ref, near_ref, others_ref, late_ref):
     tokens = token_ref[...].astype(F32)
     scale = lax.rsqrt(jnp.mean(tokens * tokens, axis=-1, keepdims=True) + NORM_EPS)
     normed = (tokens * scale * gain_ref[...]).astype(BF16)
+    rows = near_ref.shape[0]
     places = slots_of(route_ref[...], core_ref[0], experts)
-    for block, send_ref in enumerate(send_refs):
-        rows = send_ref.shape[0]
+    targets = ((near_ref, 0), (others_ref, 0), (late_ref, 0), (others_ref, rows))
+    for block, (ref, start) in enumerate(targets):
         number = lax.broadcasted_iota(jnp.int32, (rows, tokens.shape[0]), 0) + block * rows
         chosen = sum((b * rows + p == number).astype(F32) for b, p in places)
-        send_ref[...] = mm(chosen.astype(BF16), normed, 1, 0).astype(BF16)
+        ref[start : start + rows, :] = mm(chosen.astype(BF16), normed, 1, 0).astype(BF16)
 
 
 def dispatch(core, tokens, gain, routes, experts):
@@ -334,8 +335,8 @@
     return pl.pallas_call(
         functools.partial(dispatch_kernel, experts),
         in_specs=[SMEM, VMEM, VMEM, VMEM],
-        out_specs=[VMEM] * 4,
-        out_shape=[jax.ShapeDtypeStruct((rows, tokens.shape[1]), BF16)] * 4,
+        out_specs=[VMEM] * 3,
+        out_shape=[jax.ShapeDtypeStruct((n * rows, tokens.shape[1]), BF16) for n in (1, 2, 1)],
         cost_estimate=pl.CostEstimate(
             flops=8 * tokens.size * rows, bytes_accessed=10 * tokens.size, transcendentals=0
         ),
@@ -385,17 +386,35 @@
     return (up_pre + 1.0) * gate_pre * jax.nn.sigmoid(SIGMOID_SCALE * gate_pre)
 
 
+def strip_of(start, i):
+    return pl.ds(pl.multiple_of(start + i * STRIP, STRIP), STRIP)
+
+
+def copied(to_ref, to_start, from_ref, from_start, rows):
+    def step(i, _):
+        strip = from_ref[strip_of(from_start, i), :]
+        to_ref[strip_of(to_start, i), :] = strip.astype(to_ref.dtype)
+        return 0
+
+    lax.fori_loop(0, rows // STRIP, step, 0)
+
+
 def expert_kernel(pieces, me_ref, gate_ref, up_ref, down_ref, *refs):
-    row_refs, out_refs, rows_ref, total_ref = refs[:pieces], refs[pieces:-2], refs[-2], refs[-1]
+    row_refs, (out_ref, rows_ref, total_ref) = refs[:pieces], refs[pieces:]
     step = pl.program_id(0)
 
     @pl.when(step == 0)
     def _():
         start = 0
         for ref in row_refs:
-            rows_ref[start : start + ref.shape[0], :] = ref[...]
+            copied(rows_ref, start, ref, 0, ref.shape[0])
             start += ref.shape[0]
-        total_ref[...] = jnp.zeros_like(total_ref)
+
+        def cleared(i, _):
+            total_ref[strip_of(0, i), :] = jnp.zeros((STRIP, total_ref.shape[1]), F32)
+            return 0
+
+        lax.fori_loop(0, total_ref.shape[0] // STRIP, cleared, 0)
 
     rows = rows_ref[...]
     gate_pre = mm(rows, gate_ref[...], 1, 0)
@@ -405,29 +424,18 @@
 
     @pl.when(step == pl.num_programs(0) - 1)
     def _():
-        if len(out_refs) > 1:
-            start = 0
-            for ref in out_refs:
-                ref[...] = total_ref[start : start + ref.shape[0], :].astype(BF16)
-                start += ref.shape[0]
-        else:
-            (ref,) = out_refs
-            owners, per = ref.shape[0], ref.shape[1]
-            for k, by in enumerate((0, owners - 1, 1, 2)):
-                owner = lax.rem(me_ref[0] + by, owners)
-                ref[owner] = total_ref[k * per : (k + 1) * per, :].astype(BF16)
-
-
-def expert_parts(me, pieces, gate_weight, up_weight, down_weight, owners=None):
+        owners, per = out_ref.shape[0], out_ref.shape[1]
+        for k, by in enumerate((0, owners - 1, 1, 2)):
+            owner = lax.rem(me_ref[0] + by, owners)
+            copied(out_ref.at[owner], 0, total_ref, k * per, per)
+
+
+def expert_parts(me, pieces, gate_weight, up_weight, down_weight, owners):
     features, hidden = gate_weight.shape
     width = min(256, hidden)
     rows = sum(p.shape[0] for p in pieces)
     whole = [pl.BlockSpec(p.shape, lambda f: (0, 0)) for p in pieces]
-    out_specs, out_shape = whole, [jax.ShapeDtypeStruct(p.shape, BF16) for p in pieces]
-    if owners:
-        by_owner = (owners, rows // owners, features)
-        out_specs = [pl.BlockSpec(by_owner, lambda f: (0, 0, 0))]
-        out_shape = [jax.ShapeDtypeStruct(by_owner, BF16)]
+    by_owner = (owners, rows // owners, features)
     return pl.pallas_call(
         functools.partial(expert_kernel, len(pieces)),
         grid=(hidden // width,),
@@ -438,8 +446,8 @@
             pl.BlockSpec((width, features), lambda f: (f, 0)),
             *whole,
         ],
-        out_specs=out_specs,
-        out_shape=out_shape,
+        out_specs=pl.BlockSpec(by_owner, lambda f: (0, 0, 0)),
+        out_shape=jax.ShapeDtypeStruct(by_owner, BF16),
         scratch_shapes=[pltpu.VMEM((rows, features), BF16), pltpu.VMEM((rows, features), F32)],
         cost_estimate=pl.CostEstimate(
             flops=6 * rows * features * hidden,
@@ -464,9 +472,15 @@
     return own, left, right, far_low, far_high
 
 
-def summed_pieces(parts):
-    own, left, right, far_low, far_high = parts
-    half = own.shape[0] // 2
+def summed_pieces(parts, me, owners):
+    half = parts.shape[1] // 2
+
+    def rows_for(by, start=0, count=2 * half):
+        owner = lax.rem(me + by, owners)
+        return lax.dynamic_slice(parts, (owner, start, 0), (1, count, parts.shape[2]))[0]
+
+    own, left, right = rows_for(0), rows_for(owners - 1), rows_for(1)
+    far_low, far_high = rows_for(2, 0, half), rows_for(2, half, half)
     from_right = turned(far_low, "tp", -1)
     from_left = turned(far_high, "tp", 1)
     low = (left[:half].astype(F32) + from_right.astype(F32)).astype(BF16)
@@ -513,15 +527,16 @@
 
     half = mixer_output_weight.shape[0] // 2
     weight_part = lax.dynamic_slice_in_dim(mixer_output_weight, core[0] * half, half, 0)
-    weight_mine = lax.all_gather(weight_part, "tp", axis=0, tiled=False)
+    weight_left = turned(weight_part, "tp", 1)
+    weight_right = turned(weight_part, "tp", -1)
+    weight_far = turned(weight_left, "tp", 1)
+    weight_mine = jnp.concatenate((weight_left, weight_right, weight_far), axis=0)
     weight_other = turned(weight_mine, "ep_1", 1)
 
     routes_t, weights_t = jnp.transpose(routes), jnp.transpose(chosen_expert_weight)
-    near, far, late_near, late_far = dispatch(
-        core, after(second_batch_tokens, weight_part), expert_norm_gain, routes_t, n_ep
-    )
-    far = turned(far, "ep_1", 1)
-    late = late_near + turned(late_far, "ep_1", 1)
+    near, others, late_near = dispatch(core, second_batch_tokens, expert_norm_gain, routes_t, n_ep)
+    others = turned(others, "ep_1", 1)
+    far, late = others[: near.shape[0]], late_near + others[near.shape[0] :]
 
     state = mixer_states(
         forget_gate_logits, value, forget_lower_margin, position_log_decay
@@ -537,21 +552,12 @@
             rows = after(rows, (arrived, late))
         arrived = sent_over_chips(rows, chips)
         pieces = gathered_pieces(arrived)
-        if not c:
-            pieces = after(pieces, weight_mine)
-        parts = expert_parts(
-            me,
-            pieces,
-            gate_weight[0],
-            up_weight[0],
-            down_weight[0],
-            owners if c else None,
-        )
+        parts = expert_parts(me, pieces, gate_weight[0], up_weight[0], down_weight[0], owners)
         if c:
-            parts = parts[0].reshape(owners * rows.shape[0], -1)
+            parts = parts.reshape(owners * rows.shape[0], -1)
             sums.append(lax.psum_scatter(parts, "tp", scatter_dimension=0, tiled=True))
         else:
-            sums.append(summed_pieces(parts))
+            sums.append(summed_pieces(parts, me[0], owners))
 
     returned = []
     for rows in sums:
@@ -579,7 +585,7 @@
         turned(heads[owners - 1], "tp", -1),
         turned(heads[2], "tp", 2),
     )
-    first_mixer_output = project(place, heads, weight_mine, weight_other)
+    first_mixer_output = project(core, heads, mixer_output_weight, weight_mine, weight_other)
 
     back_near, back_far, back_late = returned
     base = combine(core, weights_t, routes_t, n_ep, (back_near, turned(back_far, "ep_1", 1)))

time: 424 us -> 412 us (0.972)
  waiting for transfers between devices: 145 us -> 131 us
    all_gather x1, waiting for transfers between devices: 56.9 us -> 42.1 us  [body(): gathered = lax.all_gather(chip_state, 'ep_0', axis=0, tiled=False)]
    ppermute x26 -> x28, starting transfers between devices: 43.2 us -> 53.4 us  [turned(): return lax.ppermute(x, axis, [(i, (i + by) % size) for i in range(size)])]
    ppermute x26 -> x28, waiting for transfers between devices: 65.5 us -> 71.8 us  [turned(): return lax.ppermute(x, axis, [(i, (i + by) % size) for i in range(size)])]
    all_to_all x4, starting transfers between devices: 66.3 us -> 60.4 us  [sent_over_chips(): lax.all_to_all(blocks, 'ep_0', split_axis=0, concat_axis=0, tiled=True)]
    all_to_all x4, waiting for transfers between devices: 22.1 us -> 17.2 us  [sent_over_chips(): lax.all_to_all(blocks, 'ep_0', split_axis=0, concat_axis=0, tiled=True)]
  transfers between devices with their start and end apart: 34 -> 35, of which waited for: 18 -> 18; matrix products, arithmetic and copies ran while one was open for 2% -> 3% of each run, Pallas kernels for 15% -> 13%
where the time goes in v2:
time: 412 us; the launch traced here: 410 us
  waiting for transfers between devices  131 us (32%)
  starting transfers between devices  114 us (28%)
  Pallas kernels  69.7 us (17%)
  blocking collectives  61.1 us (15%)
  between operations  15.9 us (4%)
  local copies, waits for them, and re-layouts  12.4 us (3%)
  other arithmetic  5.58 us (1%)
    ppermute x28, waiting for transfers between devices, turned(): return lax.ppermute(x, axis, [(i, (i + by) % size) for i in range(size)])  71.8 us
    all_to_all x2, blocking collectives, sent_over_chips(): lax.all_to_all(blocks, 'ep_0', split_axis=0, concat_axis=0, tiled=True)  61.1 us
    all_to_all x4, starting transfers between devices, sent_over_chips(): lax.all_to_all(blocks, 'ep_0', split_axis=0, concat_axis=0, tiled=True)  60.4 us
    ppermute x28, starting transfers between devices, turned(): return lax.ppermute(x, axis, [(i, (i + by) % size) for i in range(size)])  53.4 us
    all_gather x1, waiting for transfers between devices, body(): gathered = lax.all_gather(chip_state, 'ep_0', axis=0, tiled=False)  42.1 us
    pallas_call x3, Pallas kernels, expert_parts(): pl.pallas_call(functools.partial(expert_kernel, len(pieces)), grid=(hidde...  25.6 us
    all_to_all x4, waiting for transfers between devices, sent_over_chips(): lax.all_to_all(blocks, 'ep_0', split_axis=0, concat_axis=0, tiled=True)  17.2 us
    pallas_call x1, Pallas kernels, mixer_heads(): pl.pallas_call(heads_kernel, in_specs=[SMEM] + [VMEM] * 9, out_specs=VMEM...  13.2 us
  transfers between devices with their start and end apart: 35, of which 18 were waited for; matrix products, arithmetic and copies ran while one was open for 3% of the time, Pallas kernels for 13%

profile of v2, /device:TPU:33, one launch (start us, length us, event | category | flops | bytes accessed | tf_op | source)
XLA Modules:
  0.0 410.0 jit_solution(8473164232004239087)
XLA Ops:
  8.0 3.1 dispatch_rows.1
  11.1 24.5 %all-to-all-start = ((bf16[16,8,2048]{2,1,0:T(8,128)(2,1)}), bf16[16,8,2048]{2,1,0:T(8,128)(2,1)S(1)}, u32[]{:S(2)}, u32[]{:S(2)}) async-start(bf16[16,8,2048]{2,1,0:T(8,128)(2,1)} %bitcast.74), calls=%async_computation | async-start | bytes 1048576 | tf_op jit(solution)/shard_map/all_to_all | solution.py:497
  35.7 1.0 collective-permute-start.17
  36.7 2.5 collective-permute-done.17
  39.2 1.9 fusion.4
  41.2 17.2 %all-to-all-done = bf16[16,8,2048]{2,1,0:T(8,128)(2,1)S(1)} async-done(((bf16[16,8,2048]{2,1,0:T(8,128)(2,1)}), bf16[16,8,2048]{2,1,0:T(8,128)(2,1)S(1)}, u32[]{:S(2)}, u32[]{:S(2)}) %all-to-all-start) | async-done | bytes 524320 | tf_op jit(solution)/shard_map/all_to_all | solution.py:497
  58.4 35.3 %all_to_all.30 = bf16[16,8,2048]{2,1,0:T(8,128)(2,1)S(1)} all-to-all(bf16[16,8,2048]{2,1,0:T(8,128)(2,1)S(1)} %bitcast.56), channel_id=1, replica_groups=mesh['grp'=2,'ep_0'=16,'ep_1'=2,'tp'=4] {'ep_0'}, dimensions={0} | all-to-all | bytes 1048576 | tf_op jit(solution)/shard_map/all_to_all | solution.py:497
  93.7 1.3 collective-permute-start.18
  95.0 1.5 collective-permute-start.19
  96.6 6.6 %collective-permute-done.18.refs_1_ = bf16[128,2048]{1,0:T(8,128)(2,1)S(1)} collective-permute-done((bf16[128,2048]{1,0:T(8,128)(2,1)S(1)}, bf16[128,2048]{1,0:T(8,128)(2,1)S(1)}, u32[]{:S(2)}, u32[]{:S(2)}) %collective-permute-start.18) | collective-permute-done | bytes 524320 | tf_op jit(solution)/shard_map/ppermute | solution.py:463
  103.3 2.7 collective-permute-start.21
  106.1 6.7 %collective-permute-done.20.refs_3_ = bf16[64,2048]{1,0:T(8,128)(2,1)S(1)} collective-permute-done((bf16[64,2048]{1,0:T(8,128)(2,1)S(1)}, bf16[64,2048]{1,0:T(8,128)(2,1)S(1)}, u32[]{:S(2)}, u32[]{:S(2)}) %collective-permute-start.20) | collective-permute-done | bytes 262176 | tf_op jit(solution)/shard_map/ppermute | solution.py:463
  112.8 0.7 copy-done.22
  113.6 8.5 %expert_parts.4 = bf16[4,128,2048]{2,1,0:T(8,128)(2,1)} custom-call(s32[1]{0:T(128)} %bitcast.1.me_ref, bf16[2048,512]{1,0:T(8,128)(2,1)} %bitcast.80, bf16[2048,512]{1,0:T(8,128)(2,1)} %bitcast.83, bf16[512,2048]{1,0:T(8,128)(2,1)} %bitcast.86, bf16[128,2048]{1,0:T(8,128)(2,1)} %bitcast.73, bf16[128,2048]{1,0:T(8,128)(2,1)} %copy-done.17, ...), custom_call_target="tpu_custom_call" | custom-call | flops 3221225472 | bytes 10485760 | tf_op jit(solution)/shard_map/expert_parts/pallas_call | solution.py:439
  122.2 16.2 %all-to-all-start.2 = ((bf16[16,8,2048]{2,1,0:T(8,128)(2,1)}), bf16[16,8,2048]{2,1,0:T(8,128)(2,1)S(1)}, u32[]{:S(2)}, u32[]{:S(2)}) async-start(bf16[16,8,2048]{2,1,0:T(8,128)(2,1)} %bitcast.26), calls=%async_computation.2 | async-start | bytes 1048576 | tf_op jit(solution)/shard_map/all_to_all | solution.py:497
  138.6 2.6 collective-permute-start.10
  141.3 12.9 %collective-permute-done.9.refs_1_ = bf16[128,2048]{1,0:T(8,128)(2,1)S(1)} collective-permute-done((bf16[128,2048]{1,0:T(8,128)(2,1)S(1)}, bf16[128,2048]{1,0:T(8,128)(2,1)S(1)}, u32[]{:S(2)}, u32[]{:S(2)}) %collective-permute-start.9) | collective-permute-done | bytes 524320 | tf_op jit(solution)/shard_map/ppermute | solution.py:463
  154.3 1.3 collective-permute-done.10.refs_2_
  155.6 3.8 collective-permute-start.12
  159.5 8.7 %collective-permute-done.11.refs_3_ = bf16[64,2048]{1,0:T(8,128)(2,1)S(1)} collective-permute-done((bf16[64,2048]{1,0:T(8,128)(2,1)S(1)}, bf16[64,2048]{1,0:T(8,128)(2,1)S(1)}, u32[]{:S(2)}, u32[]{:S(2)}) %collective-permute-start.11) | collective-permute-done | bytes 262176 | tf_op jit(solution)/shard_map/ppermute | solution.py:463
  168.1 1.6 collective-permute-done.12.refs_4_
  169.7 0.7 copy-done.20
  170.4 8.6 %expert_parts.3 = bf16[4,128,2048]{2,1,0:T(8,128)(2,1)} custom-call(s32[1]{0:T(128)} %bitcast.1.me_ref, bf16[2048,512]{1,0:T(8,128)(2,1)} %bitcast.81, bf16[2048,512]{1,0:T(8,128)(2,1)} %bitcast.84, bf16[512,2048]{1,0:T(8,128)(2,1)} %bitcast.87, bf16[128,2048]{1,0:T(8,128)(2,1)} %bitcast.68, bf16[128,2048]{1,0:T(8,128)(2,1)} %copy-done.13, ...), custom_call_target="tpu_custom_call" | custom-call | flops 3221225472 | bytes 10485760 | tf_op jit(solution)/shard_map/expert_parts/pallas_call | solution.py:439
  179.0 2.2 dynamic-slice_bitcast_fusion.3
  181.2 3.5 collective-permute-start.15
  184.8 2.7 collective-permute-start.24
  187.4 1.3 collective-permute-done.13
  188.7 0.7 copy-done.8
  189.4 1.2 fusion.3
  190.6 5.3 %collective-permute-done.23.refs_1_ = bf16[128,2048]{1,0:T(8,128)(2,1)S(1)} collective-permute-done((bf16[128,2048]{1,0:T(8,128)(2,1)S(1)}, bf16[128,2048]{1,0:T(8,128)(2,1)S(1)}, u32[]{:S(2)}, u32[]{:S(2)}) %collective-permute-start.23) | collective-permute-done | bytes 524320 | tf_op jit(solution)/shard_map/ppermute | solution.py:463
  196.1 0.6 copy-done.15
  196.7 2.4 collective-permute-start.26
  199.1 0.8 pad_maximum_fusion
  199.9 0.8 pad_maximum_fusion.1
  200.8 2.7 collective-permute-start.16
  203.4 2.1 collective-permute-done.25.refs_3_
  205.6 0.7 copy-done.21
  206.3 8.6 %expert_parts.5 = bf16[4,128,2048]{2,1,0:T(8,128)(2,1)} custom-call(s32[1]{0:T(128)} %bitcast.1.me_ref, bf16[2048,512]{1,0:T(8,128)(2,1)} %bitcast.82, bf16[2048,512]{1,0:T(8,128)(2,1)} %bitcast.85, bf16[512,2048]{1,0:T(8,128)(2,1)} %bitcast.88, bf16[128,2048]{1,0:T(8,128)(2,1)} %bitcast.65, bf16[128,2048]{1,0:T(8,128)(2,1)} %copy-done.15, ...), custom_call_target="tpu_custom_call" | custom-call | flops 3221225472 | bytes 10485760 | tf_op jit(solution)/shard_map/expert_parts/pallas_call | solution.py:439
  215.2 25.8 %all_to_all.31 = bf16[16,8,2048]{2,1,0:T(8,128)(2,1)} all-to-all(bf16[16,8,2048]{2,1,0:T(8,128)(2,1)S(1)} %bitcast.57), channel_id=1, replica_groups=mesh['grp'=2,'ep_0'=16,'ep_1'=2,'tp'=4] {'ep_0'}, dimensions={0} | all-to-all | bytes 1048576 | tf_op jit(solution)/shard_map/all_to_all | solution.py:497
  241.0 7.9 %all-to-all-start.4 = ((bf16[16,8,2048]{2,1,0:T(8,128)(2,1)}), bf16[16,8,2048]{2,1,0:T(8,128)(2,1)S(1)}, u32[]{:S(2)}, u32[]{:S(2)}) async-start(bf16[16,8,2048]{2,1,0:T(8,128)(2,1)} %bitcast.62), calls=%async_computation.5 | async-start | bytes 1048576 | tf_op jit(solution)/shard_map/all_to_all | solution.py:497
  249.0 10.3 %mixer_states.1.own_ref = bf16[2,2,144,128]{3,2,1,0:T(8,128)(2,1)} custom-call(bf16[1024,256]{1,0:T(8,128)(2,1)} %logits_ref.3, bf16[1024,256]{1,0:T(8,128)(2,1)} %value_ref.3, f32[2,256]{1,0:T(2,128)} %margin_ref.3, f32[2,1024]{1,0:T(2,128)} %decay_ref.3), custom_call_target="tpu_custom_call" | custom-call | flops 805306368 | bytes 1310720 | tf_op jit(solution)/shard_map/mixer_states/pallas_call | solution.py:108
  259.3 13.0 %collective-permute-start = (bf16[2,2,144,128]{3,2,1,0:T(8,128)(2,1)}, bf16[2,2,144,128]{3,2,1,0:T(8,128)(2,1)S(1)}, u32[]{:S(2)}, u32[]{:S(2)}) collective-permute-start(bf16[2,2,144,128]{3,2,1,0:T(8,128)(2,1)} %mixer_states.1.own_ref), channel_id=1, source_target_pairs={{0,4},{4,0},{1,5},{5,1},{2,6},{6,2},{3,7},{7,3},{8,12},{12,8},{9,1... | collective-permute-start | bytes 442376 | tf_op jit(solution)/shard_map/ppermute | solution.py:463
  272.3 1.2 collective-permute-done.partner_ref
  273.5 0.7 copy-done.9
  274.2 1.7 mixer_merge.1
  275.9 0.8 constant_dynamic-slice_fusion
  276.7 2.7 collective-permute-start.6
  279.4 11.8 %all-to-all-start.5 = ((bf16[16,8,2048]{2,1,0:T(8,128)(2,1)}), bf16[16,8,2048]{2,1,0:T(8,128)(2,1)S(1)}, u32[]{:S(2)}, u32[]{:S(2)}) async-start(bf16[16,8,2048]{2,1,0:T(8,128)(2,1)} %bitcast.70), calls=%async_computation.7 | async-start | bytes 1048576 | tf_op jit(solution)/shard_map/all_to_all | solution.py:497
  291.4 1.1 constant_dynamic-update-slice_fusion.1
  292.5 12.4 %collective-permute-done.7 = bf16[128,2048]{1,0:T(8,128)(2,1)S(1)} collective-permute-done((bf16[128,2048]{1,0:T(8,128)(2,1)S(1)}, bf16[128,2048]{1,0:T(8,128)(2,1)S(1)}, u32[]{:S(2)}, u32[]{:S(2)}) %collective-permute-start.7) | collective-permute-done | bytes 524320 | tf_op jit(solution)/shard_map/ppermute | solution.py:463
  304.9 2.1 collective-permute-start.8
  307.0 42.1 %all-gather.3.cloned.1.call-done = bf16[32,144,128]{2,1,0:T(8,128)(2,1)} async-done(((bf16[2,144,128]{2,1,0:T(8,128)(2,1)}), bf16[32,144,128]{2,1,0:T(8,128)(2,1)}) %all-gather.3.cloned.1.call-update) | async-done | bytes 1179664 | tf_op jit(solution)/shard_map/all_gather | solution.py:546
  349.1 2.6 mixer_entering.1.mine_ref
  351.7 7.6 %collective-permute-start.1 = (bf16[2,128,128]{2,1,0:T(8,128)(2,1)}, bf16[2,128,128]{2,1,0:T(8,128)(2,1)S(1)}, u32[]{:S(2)}, u32[]{:S(2)}) collective-permute-start(bf16[2,128,128]{2,1,0:T(8,128)(2,1)} %mixer_entering.1.mine_ref), channel_id=1, source_target_pairs={{0,4},{4,0},{1,5},{5,1},{2,6},{6,2},{3,7},{7,3},{8,12},{12,8},{9,1... | collective-permute-start | bytes 196616 | tf_op jit(solution)/shard_map/ppermute | solution.py:463
  361.0 13.2 %mixer_heads.1 = bf16[4,2,256,128]{3,2,1,0:T(8,128)(2,1)} custom-call(s32[2]{0:T(128)} %pad_add_fusion.place_ref, bf16[1024,256]{1,0:T(8,128)(2,1)} %query_ref.1, bf16[1024,256]{1,0:T(8,128)(2,1)} %logits_ref.3, bf16[1024,256]{1,0:T(8,128)(2,1)} %value_ref.3, f32[2,256]{1,0:T(2,128)} %margin_ref.3, f32[2,1024]{1,0:T(2,128)} %decay_ref.3, f32[1,128]{1,0:T(1,128)} %bitcast.90, ...), custom_call_target="tpu_custom_call" | custom-call | flops 1610612736 | bytes 4194304 | tf_op jit(solution)/shard_map/mixer_heads/pallas_call | solution.py:256
  374.7 1.8 slice_bitcast_fusion
  376.5 2.7 collective-permute-start.3
  379.2 3.3 collective-permute-done.2.left_ref
  382.5 5.3 %collective-permute-done.4.far_ref = bf16[2,256,128]{2,1,0:T(8,128)(2,1)S(1)} collective-permute-done((bf16[2,256,128]{2,1,0:T(8,128)(2,1)S(1)}, bf16[2,256,128]{2,1,0:T(8,128)(2,1)S(1)}, u32[]{:S(2)}, u32[]{:S(2)}) %collective-permute-start.4) | collective-permute-done | bytes 131104 | tf_op jit(solution)/shard_map/ppermute | solution.py:463
  387.8 0.6 copy-done.12
  388.5 6.9 %mixer_project.1 = bf16[256,2048]{1,0:T(8,128)(2,1)} custom-call(s32[1]{0:T(128)} %bitcast.core_ref, bf16[2,256,128]{2,1,0:T(8,128)(2,1)} %get-tuple-element.29.own_ref, bf16[2,256,128]{2,1,0:T(8,128)(2,1)} %copy-done.10, bf16[2,256,128]{2,1,0:T(8,128)(2,1)} %copy-done.11, bf16[2,256,128]{2,1,0:T(8,128)(2,1)} %copy-done.12, bf16[256,2048]{1,0:T(8,128)(2,1)} %weight_ref.1, ...), custom_call_target="tpu_custom_call" | custom-call | flops 1073741824 | bytes 4194304 | tf_op jit(solution)/shard_map/mixer_project/pallas_call | solution.py:288
  395.4 3.1 combine_rows.2.refs_0_
  398.5 0.8 copy-done.4
  399.3 3.2 combine_rows.3
  (90 shorter events, 3.9 us)
Async XLA Ops:
  11.1 47.3 %all-to-all-start = ((bf16[16,8,2048]{2,1,0:T(8,128)(2,1)}), bf16[16,8,2048]{2,1,0:T(8,128)(2,1)S(1)}, u32[]{:S(2)}, u32[]{:S(2)}) async-start(bf16[16,8,2048]{2,1,0:T(8,128)(2,1)} %bitcast.74), calls=%async_computation | async-start | bytes 1048576 | tf_op jit(solution)/shard_map/all_to_all | solution.py:497
  35.7 205.3 %reduce-scatter.3.cloned.1.call-start = ((), (), s32[]{:S(2)}) async-start(), calls=%async_computation.8 | async-start | bytes 2621440 | tf_op jit(solution)/shard_map/reduce_scatter | solution.py:558
  35.7 3.5 collective-permute-start.17
  58.4 80.2 %copy-start.6 = (bf16[16,8,2048]{2,1,0:T(8,128)(2,1)}, bf16[16,8,2048]{2,1,0:T(8,128)(2,1)S(1)}, u32[]{:S(2)}) copy-start(bf16[16,8,2048]{2,1,0:T(8,128)(2,1)S(1)} %all-to-all-done) | copy-start | bytes 1572868
  93.7 19.1 %copy-start.7 = (bf16[16,8,2048]{2,1,0:T(8,128)(2,1)}, bf16[16,8,2048]{2,1,0:T(8,128)(2,1)S(1)}, u32[]{:S(2)}) copy-start(bf16[16,8,2048]{2,1,0:T(8,128)(2,1)S(1)} %all_to_all.30) | copy-start | bytes 1572868
  93.7 9.5 %collective-permute-start.18 = (bf16[128,2048]{1,0:T(8,128)(2,1)S(1)}, bf16[128,2048]{1,0:T(8,128)(2,1)S(1)}, u32[]{:S(2)}, u32[]{:S(2)}) collective-permute-start(bf16[128,2048]{1,0:T(8,128)(2,1)S(1)} %bitcast.71), channel_id=1, source_target_pairs={{0,1},{1,2},{2,3},{3,0},{4,5},{5,6},{6,7},{7,4},{8,9},{9,10},{10,1... | collective-permute-start | bytes 1572872 | tf_op jit(solution)/shard_map/ppermute | solution.py:463
  95.0 8.3 %collective-permute-start.19 = (bf16[128,2048]{1,0:T(8,128)(2,1)S(1)}, bf16[128,2048]{1,0:T(8,128)(2,1)S(1)}, u32[]{:S(2)}, u32[]{:S(2)}) collective-permute-start(bf16[128,2048]{1,0:T(8,128)(2,1)S(1)} %bitcast.72), channel_id=1, source_target_pairs={{0,3},{1,0},{2,1},{3,2},{4,7},{5,4},{6,5},{7,6},{8,11},{9,8},{10,9... | collective-permute-start | bytes 1572872 | tf_op jit(solution)/shard_map/ppermute | solution.py:463
  103.1 9.7 %copy-start.17 = (bf16[128,2048]{1,0:T(8,128)(2,1)}, bf16[128,2048]{1,0:T(8,128)(2,1)S(1)}, u32[]{:S(2)}) copy-start(bf16[128,2048]{1,0:T(8,128)(2,1)S(1)} %collective-permute-done.18.refs_1_) | copy-start | bytes 1572868
  103.2 9.6 %collective-permute-start.20 = (bf16[64,2048]{1,0:T(8,128)(2,1)S(1)}, bf16[64,2048]{1,0:T(8,128)(2,1)S(1)}, u32[]{:S(2)}, u32[]{:S(2)}) collective-permute-start(bf16[64,2048]{1,0:T(8,128)(2,1)S(1)} %slice.82), channel_id=1, source_target_pairs={{0,1},{1,2},{2,3},{3,0},{4,5},{5,6},{6,7},{7,4},{8,9},{9,10},{10,1... | collective-permute-start | bytes 786440 | tf_op jit(solution)/shard_map/ppermute | solution.py:463
  103.3 9.5 %copy-start.18 = (bf16[128,2048]{1,0:T(8,128)(2,1)}, bf16[128,2048]{1,0:T(8,128)(2,1)S(1)}, u32[]{:S(2)}) copy-start(bf16[128,2048]{1,0:T(8,128)(2,1)S(1)} %collective-permute-done.19.refs_2_) | copy-start | bytes 1572868
  103.3 9.5 %collective-permute-start.21 = (bf16[64,2048]{1,0:T(8,128)(2,1)S(1)}, bf16[64,2048]{1,0:T(8,128)(2,1)S(1)}, u32[]{:S(2)}, u32[]{:S(2)}) collective-permute-start(bf16[64,2048]{1,0:T(8,128)(2,1)S(1)} %slice.83), channel_id=1, source_target_pairs={{0,3},{1,0},{2,1},{3,2},{4,7},{5,4},{6,5},{7,6},{8,11},{9,8},{10,9... | collective-permute-start | bytes 786440 | tf_op jit(solution)/shard_map/ppermute | solution.py:463
  112.8 0.7 copy-start.22
  112.8 0.8 copy-start.23
  122.2 62.6 %all-to-all-start.2 = ((bf16[16,8,2048]{2,1,0:T(8,128)(2,1)}), bf16[16,8,2048]{2,1,0:T(8,128)(2,1)S(1)}, u32[]{:S(2)}, u32[]{:S(2)}) async-start(bf16[16,8,2048]{2,1,0:T(8,128)(2,1)} %bitcast.26), calls=%async_computation.2 | async-start | bytes 1048576 | tf_op jit(solution)/shard_map/all_to_all | solution.py:497
  138.4 141.0 %reduce-scatter.5.cloned.1.call-start = ((), (), s32[]{:S(2)}) async-start(), calls=%async_computation.9 | async-start | bytes 2621440 | tf_op jit(solution)/shard_map/reduce_scatter | solution.py:558
  138.5 15.7 %collective-permute-start.9 = (bf16[128,2048]{1,0:T(8,128)(2,1)S(1)}, bf16[128,2048]{1,0:T(8,128)(2,1)S(1)}, u32[]{:S(2)}, u32[]{:S(2)}) collective-permute-start(bf16[128,2048]{1,0:T(8,128)(2,1)S(1)} %bitcast.66), channel_id=1, source_target_pairs={{0,1},{1,2},{2,3},{3,0},{4,5},{5,6},{6,7},{7,4},{8,9},{9,10},{10,1... | collective-permute-start | bytes 1572872 | tf_op jit(solution)/shard_map/ppermute | solution.py:463
  138.6 17.0 %collective-permute-start.10 = (bf16[128,2048]{1,0:T(8,128)(2,1)S(1)}, bf16[128,2048]{1,0:T(8,128)(2,1)S(1)}, u32[]{:S(2)}, u32[]{:S(2)}) collective-permute-start(bf16[128,2048]{1,0:T(8,128)(2,1)S(1)} %bitcast.67), channel_id=1, source_target_pairs={{0,3},{1,0},{2,1},{3,2},{4,7},{5,4},{6,5},{7,6},{8,11},{9,8},{10,9... | collective-permute-start | bytes 1572872 | tf_op jit(solution)/shard_map/ppermute | solution.py:463
  154.1 15.6 %copy-start.13 = (bf16[128,2048]{1,0:T(8,128)(2,1)}, bf16[128,2048]{1,0:T(8,128)(2,1)S(1)}, u32[]{:S(2)}) copy-start(bf16[128,2048]{1,0:T(8,128)(2,1)S(1)} %collective-permute-done.9.refs_1_) | copy-start | bytes 1572868
  154.2 14.0 %collective-permute-start.11 = (bf16[64,2048]{1,0:T(8,128)(2,1)S(1)}, bf16[64,2048]{1,0:T(8,128)(2,1)S(1)}, u32[]{:S(2)}, u32[]{:S(2)}) collective-permute-start(bf16[64,2048]{1,0:T(8,128)(2,1)S(1)} %slice.78), channel_id=1, source_target_pairs={{0,1},{1,2},{2,3},{3,0},{4,5},{5,6},{6,7},{7,4},{8,9},{9,10},{10,1... | collective-permute-start | bytes 786440 | tf_op jit(solution)/shard_map/ppermute | solution.py:463
  155.6 14.1 %copy-start.14 = (bf16[128,2048]{1,0:T(8,128)(2,1)}, bf16[128,2048]{1,0:T(8,128)(2,1)S(1)}, u32[]{:S(2)}) copy-start(bf16[128,2048]{1,0:T(8,128)(2,1)S(1)} %collective-permute-done.10.refs_2_) | copy-start | bytes 1572868
  155.6 14.1 %collective-permute-start.12 = (bf16[64,2048]{1,0:T(8,128)(2,1)S(1)}, bf16[64,2048]{1,0:T(8,128)(2,1)S(1)}, u32[]{:S(2)}, u32[]{:S(2)}) collective-permute-start(bf16[64,2048]{1,0:T(8,128)(2,1)S(1)} %slice.79), channel_id=1, source_target_pairs={{0,3},{1,0},{2,1},{3,2},{4,7},{5,4},{6,5},{7,6},{8,11},{9,8},{10,9... | collective-permute-start | bytes 786440 | tf_op jit(solution)/shard_map/ppermute | solution.py:463
  168.1 1.6 copy-start.19
  169.7 0.7 copy-start.20
  179.0 10.4 %copy-start.2 = (bf16[4,128,2048]{2,1,0:T(8,128)(2,1)S(1)}, bf16[4,128,2048]{2,1,0:T(8,128)(2,1)}, u32[]{:S(2)}) copy-start(bf16[4,128,2048]{2,1,0:T(8,128)(2,1)} %expert_parts.3) | copy-start | bytes 6291460
  181.2 7.5 %collective-permute-start.13 = (bf16[64,2048]{1,0:T(8,128)(2,1)}, bf16[64,2048]{1,0:T(8,128)(2,1)S(1)}, u32[]{:S(2)}, u32[]{:S(2)}) collective-permute-start(bf16[64,2048]{1,0:T(8,128)(2,1)} %get-tuple-element.21), channel_id=1, source_target_pairs={{0,1},{1,2},{2,3},{3,0},{4,5},{5,6},{6,7},{7,4},{8,9},{9,10},{10,1... | collective-permute-start | bytes 786440 | tf_op jit(solution)/shard_map/ppermute | solution.py:463
  181.2 8.2 %collective-permute-start.15 = (bf16[64,2048]{1,0:T(8,128)(2,1)}, bf16[64,2048]{1,0:T(8,128)(2,1)}, u32[]{:S(2)}, u32[]{:S(2)}) collective-permute-start(bf16[64,2048]{1,0:T(8,128)(2,1)} %get-tuple-element.19), channel_id=1, source_target_pairs={{0,3},{1,0},{2,1},{3,2},{4,7},{5,4},{6,5},{7,6},{8,11},{9,8},{10,9... | collective-permute-start | bytes 786440 | tf_op jit(solution)/shard_map/ppermute | solution.py:463
  184.8 15.2 %copy-start.5 = (bf16[16,8,2048]{2,1,0:T(8,128)(2,1)}, bf16[16,8,2048]{2,1,0:T(8,128)(2,1)S(1)}, u32[]{:S(2)}) copy-start(bf16[16,8,2048]{2,1,0:T(8,128)(2,1)S(1)} %all-to-all-done.2) | copy-start | bytes 1572868
  184.8 11.1 %collective-permute-start.23 = (bf16[128,2048]{1,0:T(8,128)(2,1)S(1)}, bf16[128,2048]{1,0:T(8,128)(2,1)S(1)}, u32[]{:S(2)}, u32[]{:S(2)}) collective-permute-start(bf16[128,2048]{1,0:T(8,128)(2,1)S(1)} %bitcast.63), channel_id=1, source_target_pairs={{0,1},{1,2},{2,3},{3,0},{4,5},{5,6},{6,7},{7,4},{8,9},{9,10},{10,1... | collective-permute-start | bytes 1572872 | tf_op jit(solution)/shard_map/ppermute | solution.py:463
  184.8 11.9 %collective-permute-start.24 = (bf16[128,2048]{1,0:T(8,128)(2,1)S(1)}, bf16[128,2048]{1,0:T(8,128)(2,1)S(1)}, u32[]{:S(2)}, u32[]{:S(2)}) collective-permute-start(bf16[128,2048]{1,0:T(8,128)(2,1)S(1)} %bitcast.64), channel_id=1, source_target_pairs={{0,3},{1,0},{2,1},{3,2},{4,7},{5,4},{6,5},{7,6},{8,11},{9,8},{10,9... | collective-permute-start | bytes 1572872 | tf_op jit(solution)/shard_map/ppermute | solution.py:463
  188.7 0.7 copy-start.8
  195.9 0.8 copy-start.15
  195.9 9.6 %collective-permute-start.25 = (bf16[64,2048]{1,0:T(8,128)(2,1)S(1)}, bf16[64,2048]{1,0:T(8,128)(2,1)S(1)}, u32[]{:S(2)}, u32[]{:S(2)}) collective-permute-start(bf16[64,2048]{1,0:T(8,128)(2,1)S(1)} %slice.84), channel_id=1, source_target_pairs={{0,1},{1,2},{2,3},{3,0},{4,5},{5,6},{6,7},{7,4},{8,9},{9,10},{10,1... | collective-permute-start | bytes 786440 | tf_op jit(solution)/shard_map/ppermute | solution.py:463
  196.7 8.9 %copy-start.16 = (bf16[128,2048]{1,0:T(8,128)(2,1)}, bf16[128,2048]{1,0:T(8,128)(2,1)S(1)}, u32[]{:S(2)}) copy-start(bf16[128,2048]{1,0:T(8,128)(2,1)S(1)} %collective-permute-done.24.refs_2_) | copy-start | bytes 1572868
  196.7 9.5 %collective-permute-start.26 = (bf16[64,2048]{1,0:T(8,128)(2,1)S(1)}, bf16[64,2048]{1,0:T(8,128)(2,1)}, u32[]{:S(2)}, u32[]{:S(2)}) collective-permute-start(bf16[64,2048]{1,0:T(8,128)(2,1)S(1)} %slice.85), channel_id=1, source_target_pairs={{0,3},{1,0},{2,1},{3,2},{4,7},{5,4},{6,5},{7,6},{8,11},{9,8},{10,9... | collective-permute-start | bytes 786440 | tf_op jit(solution)/shard_map/ppermute | solution.py:463
  199.9 15.0 %collective-permute-start.14 = (bf16[128,2048]{1,0:T(8,128)(2,1)}, bf16[128,2048]{1,0:T(8,128)(2,1)S(1)}, u32[]{:S(2)}, u32[]{:S(2)}) collective-permute-start(bf16[128,2048]{1,0:T(8,128)(2,1)} %pad_maximum_fusion), channel_id=1, source_target_pairs={{0,1},{1,2},{2,3},{3,0},{4,5},{5,6},{6,7},{7,4},{8,9},{9,10},{10,1... | collective-permute-start | bytes 1572872 | tf_op jit(solution)/shard_map/ppermute | solution.py:463
  200.8 14.2 %collective-permute-start.16 = (bf16[128,2048]{1,0:T(8,128)(2,1)}, bf16[128,2048]{1,0:T(8,128)(2,1)S(1)}, u32[]{:S(2)}, u32[]{:S(2)}) collective-permute-start(bf16[128,2048]{1,0:T(8,128)(2,1)} %pad_maximum_fusion.1), channel_id=1, source_target_pairs={{0,3},{1,0},{2,1},{3,2},{4,7},{5,4},{6,5},{7,6},{8,11},{9,8},{10,9... | collective-permute-start | bytes 1572872 | tf_op jit(solution)/shard_map/ppermute | solution.py:463
  205.6 0.7 copy-start.21
  241.0 38.4 %all-to-all-start.4 = ((bf16[16,8,2048]{2,1,0:T(8,128)(2,1)}), bf16[16,8,2048]{2,1,0:T(8,128)(2,1)S(1)}, u32[]{:S(2)}, u32[]{:S(2)}) async-start(bf16[16,8,2048]{2,1,0:T(8,128)(2,1)} %bitcast.62), calls=%async_computation.5 | async-start | bytes 1048576 | tf_op jit(solution)/shard_map/all_to_all | solution.py:497
  248.9 27.0 %copy-start.1 = (bf16[256,2048]{1,0:T(8,128)(2,1)S(1)}, bf16[256,2048]{1,0:T(8,128)(2,1)}, u32[]{:S(2)}) copy-start(bf16[256,2048]{1,0:T(8,128)(2,1)} %weight_ref.1) | copy-start | bytes 3145732
  248.9 100.2 %all-gather.3.cloned.1.call-start = ((), (), s32[]{:S(2)}) async-start(), calls=%async_computation.10 | async-start | bytes 1253376 | tf_op jit(solution)/shard_map/all_gather | solution.py:546
  259.3 14.2 %collective-permute-start = (bf16[2,2,144,128]{3,2,1,0:T(8,128)(2,1)}, bf16[2,2,144,128]{3,2,1,0:T(8,128)(2,1)S(1)}, u32[]{:S(2)}, u32[]{:S(2)}) collective-permute-start(bf16[2,2,144,128]{3,2,1,0:T(8,128)(2,1)} %mixer_states.1.own_ref), channel_id=1, source_target_pairs={{0,4},{4,0},{1,5},{5,1},{2,6},{6,2},{3,7},{7,3},{8,12},{12,8},{9,1... | collective-permute-start | bytes 442376 | tf_op jit(solution)/shard_map/ppermute | solution.py:463
  273.5 0.7 copy-start.9
  276.7 14.5 %collective-permute-start.5 = (bf16[128,2048]{1,0:T(8,128)(2,1)}, bf16[128,2048]{1,0:T(8,128)(2,1)S(1)}, u32[]{:S(2)}, u32[]{:S(2)}) collective-permute-start(bf16[128,2048]{1,0:T(8,128)(2,1)} %constant_dynamic-slice_fusion), channel_id=1, source_target_pairs={{0,1},{1,2},{2,3},{3,0},{4,5},{5,6},{6,7},{7,4},{8,9},{9,10},{10,1... | collective-permute-start | bytes 1572872 | tf_op jit(solution)/shard_map/ppermute | solution.py:463
  276.7 14.6 %collective-permute-start.6 = (bf16[128,2048]{1,0:T(8,128)(2,1)}, bf16[128,2048]{1,0:T(8,128)(2,1)}, u32[]{:S(2)}, u32[]{:S(2)}) collective-permute-start(bf16[128,2048]{1,0:T(8,128)(2,1)} %constant_dynamic-slice_fusion), channel_id=1, source_target_pairs={{0,3},{1,0},{2,1},{3,2},{4,7},{5,4},{6,5},{7,6},{8,11},{9,8},{10,9... | collective-permute-start | bytes 1572872 | tf_op jit(solution)/shard_map/ppermute | solution.py:463
  279.4 95.2 %all-to-all-start.5 = ((bf16[16,8,2048]{2,1,0:T(8,128)(2,1)}), bf16[16,8,2048]{2,1,0:T(8,128)(2,1)S(1)}, u32[]{:S(2)}, u32[]{:S(2)}) async-start(bf16[16,8,2048]{2,1,0:T(8,128)(2,1)} %bitcast.70), calls=%async_computation.7 | async-start | bytes 1048576 | tf_op jit(solution)/shard_map/all_to_all | solution.py:497
  291.3 13.6 %collective-permute-start.7 = (bf16[128,2048]{1,0:T(8,128)(2,1)S(1)}, bf16[128,2048]{1,0:T(8,128)(2,1)S(1)}, u32[]{:S(2)}, u32[]{:S(2)}) collective-permute-start(bf16[128,2048]{1,0:T(8,128)(2,1)S(1)} %collective-permute-done.5), channel_id=1, source_target_pairs={{0,1},{1,2},{2,3},{3,0},{4,5},{5,6},{6,7},{7,4},{8,9},{9,10},{10,1... | collective-permute-start | bytes 1572872 | tf_op jit(solution)/shard_map/ppermute | solution.py:463
  304.9 69.3 %copy-start = (bf16[384,2048]{1,0:T(8,128)(2,1)}, bf16[384,2048]{1,0:T(8,128)(2,1)S(1)}, u32[]{:S(2)}) copy-start(bf16[384,2048]{1,0:T(8,128)(2,1)S(1)} %constant_dynamic-update-slice_fusion.mine_ref) | copy-start | bytes 4718596
  304.9 82.9 %collective-permute-start.8 = (bf16[384,2048]{1,0:T(8,128)(2,1)S(1)}, bf16[384,2048]{1,0:T(8,128)(2,1)}, u32[]{:S(2)}, u32[]{:S(2)}) collective-permute-start(bf16[384,2048]{1,0:T(8,128)(2,1)S(1)} %constant_dynamic-update-slice_fusion.mine_ref), channel_id=1, source_target_pairs={{0,4},{4,0},{1,5},{5,1},{2,6},{6,2},{3,7},{7,3},{8,12},{12,8},{9,1... | collective-permute-start | bytes 4718600 | tf_op jit(solution)/shard_map/ppermute | solution.py:463
  351.7 8.7 %collective-permute-start.1 = (bf16[2,128,128]{2,1,0:T(8,128)(2,1)}, bf16[2,128,128]{2,1,0:T(8,128)(2,1)S(1)}, u32[]{:S(2)}, u32[]{:S(2)}) collective-permute-start(bf16[2,128,128]{2,1,0:T(8,128)(2,1)} %mixer_entering.1.mine_ref), channel_id=1, source_target_pairs={{0,4},{4,0},{1,5},{5,1},{2,6},{6,2},{3,7},{7,3},{8,12},{12,8},{9,1... | collective-permute-start | bytes 196616 | tf_op jit(solution)/shard_map/ppermute | solution.py:463
  360.4 0.6 copy-start.24
  374.2 21.2 %collective-permute-start.22 = (bf16[128,2048]{1,0:T(8,128)(2,1)S(1)}, bf16[128,2048]{1,0:T(8,128)(2,1)}, u32[]{:S(2)}, u32[]{:S(2)}) collective-permute-start(bf16[128,2048]{1,0:T(8,128)(2,1)S(1)} %bitcast.69), channel_id=1, source_target_pairs={{0,4},{4,0},{1,5},{5,1},{2,6},{6,2},{3,7},{7,3},{8,12},{12,8},{9,1... | collective-permute-start | bytes 1572872 | tf_op jit(solution)/shard_map/ppermute | solution.py:463
  374.6 20.8 %copy-start.3 = (bf16[16,8,2048]{2,1,0:T(8,128)(2,1)}, bf16[16,8,2048]{2,1,0:T(8,128)(2,1)S(1)}, u32[]{:S(2)}) copy-start(bf16[16,8,2048]{2,1,0:T(8,128)(2,1)S(1)} %all-to-all-done.5) | copy-start | bytes 1572868
  374.6 23.9 %collective-permute-start.27 = (bf16[128,2048]{1,0:T(8,128)(2,1)S(1)}, bf16[128,2048]{1,0:T(8,128)(2,1)S(1)}, u32[]{:S(2)}, u32[]{:S(2)}) collective-permute-start(bf16[128,2048]{1,0:T(8,128)(2,1)S(1)} %bitcast.54), channel_id=1, source_target_pairs={{0,4},{4,0},{1,5},{5,1},{2,6},{6,2},{3,7},{7,3},{8,12},{12,8},{9,1... | collective-permute-start | bytes 1572872 | tf_op jit(solution)/shard_map/ppermute | solution.py:463
  376.5 5.9 %collective-permute-start.2 = (bf16[2,256,128]{2,1,0:T(8,128)(2,1)S(1)}, bf16[2,256,128]{2,1,0:T(8,128)(2,1)S(1)}, u32[]{:S(2)}, u32[]{:S(2)}) collective-permute-start(bf16[2,256,128]{2,1,0:T(8,128)(2,1)S(1)} %get-tuple-element.28), channel_id=1, source_target_pairs={{0,1},{1,2},{2,3},{3,0},{4,5},{5,6},{6,7},{7,4},{8,9},{9,10},{10,1... | collective-permute-start | bytes 393224 | tf_op jit(solution)/shard_map/ppermute | solution.py:463
  376.5 6.0 %collective-permute-start.3 = (bf16[2,256,128]{2,1,0:T(8,128)(2,1)S(1)}, bf16[2,256,128]{2,1,0:T(8,128)(2,1)S(1)}, u32[]{:S(2)}, u32[]{:S(2)}) collective-permute-start(bf16[2,256,128]{2,1,0:T(8,128)(2,1)S(1)} %get-tuple-element.27), channel_id=1, source_target_pairs={{0,3},{1,0},{2,1},{3,2},{4,7},{5,4},{6,5},{7,6},{8,11},{9,8},{10,9... | collective-permute-start | bytes 393224 | tf_op jit(solution)/shard_map/ppermute | solution.py:463
  382.5 5.3 %copy-start.10 = (bf16[2,256,128]{2,1,0:T(8,128)(2,1)}, bf16[2,256,128]{2,1,0:T(8,128)(2,1)S(1)}, u32[]{:S(2)}) copy-start(bf16[2,256,128]{2,1,0:T(8,128)(2,1)S(1)} %collective-permute-done.2.left_ref) | copy-start | bytes 393220
  382.5 5.3 %collective-permute-start.4 = (bf16[2,256,128]{2,1,0:T(8,128)(2,1)S(1)}, bf16[2,256,128]{2,1,0:T(8,128)(2,1)S(1)}, u32[]{:S(2)}, u32[]{:S(2)}) collective-permute-start(bf16[2,256,128]{2,1,0:T(8,128)(2,1)S(1)} %get-tuple-element.26), channel_id=1, source_target_pairs={{0,2},{1,3},{2,0},{3,1},{4,6},{5,7},{6,4},{7,5},{8,10},{9,11},{10,... | collective-permute-start | bytes 393224 | tf_op jit(solution)/shard_map/ppermute | solution.py:463
  382.5 5.3 %copy-start.11 = (bf16[2,256,128]{2,1,0:T(8,128)(2,1)}, bf16[2,256,128]{2,1,0:T(8,128)(2,1)S(1)}, u32[]{:S(2)}) copy-start(bf16[2,256,128]{2,1,0:T(8,128)(2,1)S(1)} %collective-permute-done.3.right_ref) | copy-start | bytes 393220
  387.8 0.7 copy-start.12
  398.5 0.8 copy-start.4
Sparse Core Ops, SparseCore 0:
  122.3 54.4 reduce-scatter.2
  215.0 44.8 reduce-scatter.4
Sparse Core Ops, SparseCore 1:
  276.0 73.1 all-gather.2
